TPU v7x, 32 devices: a whole 2x2x4 slice. The times are simulated.
32 devices in a mesh: vp: 8 (over z, x), dp: 4 (over y, core).
Axes of the slice: x: 2, y: 2, z: 4, core: 2. Of those that a mesh axis runs over, the one named last changes fastest.
Arguments:
- stream: bfloat16 [1024, 2048], P(('dp', 'vp')), may hold values from -60 to 60
- hidden: bfloat16 [1024, 5632], P('dp', 'vp'), may hold values from -6 to 6
- w_down: bfloat16 [5632, 2048], P(None, 'vp'), may hold values from -0.078125 to 0.078125
- final_gain: float32 [2048], replicated, may hold values from 0.1 to 1.9
- vocab: bfloat16 [2048, 32768], P(None, 'vp'), may hold values from -2 to 200
- vocab_bias: float32 [32768], P('vp'), may hold values from -5 to 5
- targets: int32 [1024], P('dp'), may hold values from 0 to 32767
Outputs:
- losses: float32 [1024], P(('dp', 'vp'))
- grad_input: float32 [1024, 2048], P(('dp', 'vp'))
- grad_vocab: float32 [2048, 32768], P('dp', 'vp')
All inputs are finite; a program needn't handle non-finite values.
Results may differ from a plain program's by a relative error of at most 0.02.
Values may be sent and summed in bfloat16 or wider, within the bound.
A program may use at most 128 MiB of HBM per device.

v0:
```python
import functools

import jax
import jax.numpy as jnp
from jax import lax
from jax.experimental import pallas as pl
from jax.experimental.pallas import tpu as pltpu
from jax.sharding import PartitionSpec as P

norm_eps = 1e-06
zloss_weight = 0.001


def combined_all(value, axis, join):
    pieces = jax.tree.map(lambda part: lax.all_gather(part, axis), value)
    head = jax.tree.map(lambda part: part[0], pieces)
    tail = jax.tree.map(lambda part: part[1:], pieces)
    total, _ = lax.scan(lambda total, section: (join(total, section), None), head, tail)
    return total


def combine_stats(first, second):
    top = jnp.maximum(first[0], second[0])
    total = first[1] * jnp.exp(first[0] - top) + second[1] * jnp.exp(second[0] - top)
    return (top, total, first[2] + second[2])


def body(stream, hidden, w_down, final_gain, vocab, vocab_bias, targets):
    rows_dev = stream.shape[0]
    width = stream.shape[1]
    group = targets.shape[0]
    mine = lax.axis_index("vp")
    feat_cols = w_down.shape[1]
    proj = jnp.dot(
        lax.all_gather(hidden, "vp", axis=1, tiled=True), w_down, preferred_element_type=jnp.float32
    )
    stream_cols = lax.all_to_all(stream, "vp", split_axis=1, concat_axis=0, tiled=True)
    normin_cols = (stream_cols.astype(jnp.float32) + proj).astype(jnp.bfloat16)
    col_values = normin_cols.astype(jnp.float32)
    square_total = lax.psum(jnp.sum(col_values * col_values, axis=1), "vp")
    inv_group = lax.rsqrt(square_total / width + norm_eps)
    gain_cols = lax.dynamic_slice_in_dim(final_gain, mine * feat_cols, feat_cols)
    normed_cols = (col_values * inv_group[:, None] * gain_cols).astype(jnp.bfloat16)
    normed = lax.all_gather(normed_cols, "vp", axis=1, tiled=True)
    normin = lax.all_to_all(normin_cols, "vp", split_axis=0, concat_axis=1, tiled=True)
    values = normin.astype(jnp.float32)
    inv = lax.rsqrt(jnp.mean(values * values, axis=1, keepdims=True) + norm_eps)
    ncols = vocab.shape[1]
    scores = jnp.dot(normed, vocab, preferred_element_type=jnp.float32) + vocab_bias
    local_top = jnp.max(scores, axis=1)
    local_total = jnp.sum(jnp.exp(scores - local_top[:, None]), axis=1)
    column_ids = lax.broadcasted_iota(jnp.int32, (group, ncols), 1) + mine * ncols
    hit = column_ids == targets[:, None]
    local_target = jnp.sum(jnp.where(hit, scores, 0.0), axis=1)
    top, total, target_score = combined_all(
        (local_top, local_total, local_target), "vp", combine_stats
    )
    lse = top + jnp.log(total)
    group_losses = lse - target_score + zloss_weight * lse * lse
    losses = lax.dynamic_slice_in_dim(group_losses, mine * rows_dev, rows_dev)
    probs = jnp.exp(scores - lse[:, None])
    dscore = (probs * (1.0 + 2.0 * zloss_weight * lse)[:, None] - jnp.where(hit, 1.0, 0.0)).astype(
        jnp.bfloat16
    )
    feat_group = width // lax.axis_size("dp")
    feat_start = lax.axis_index("dp") * feat_group
    rows_slice = lax.dynamic_slice_in_dim(
        lax.all_gather(normed, "dp", axis=0, tiled=True), feat_start, feat_group, 1
    )
    grad_vocab = lax.dot_general(
        rows_slice,
        lax.all_gather(dscore, "dp", axis=0, tiled=True),
        (((0,), (0,)), ((), ())),
        preferred_element_type=jnp.float32,
    )
    row_term = lax.dot_general(
        dscore, vocab, (((1,), (1,)), ((), ())), preferred_element_type=jnp.float32
    )
    row_parts = lax.all_to_all(
        row_term[:, None, :].astype(jnp.bfloat16), "vp", split_axis=0, concat_axis=1, tiled=True
    ).astype(jnp.float32)
    dnormed = jnp.sum(row_parts, axis=1)
    scaled = dnormed * final_gain
    grad_input = inv * (
        scaled - values * inv * inv * jnp.mean(values * scaled, axis=1, keepdims=True)
    )
    return (losses, grad_input, grad_vocab)


MESH = pl.DeviceIdType.MESH
HALVES = 2
TILE = 512


def send(src, dst, send_sem, recv_sem, vp, dp):
    return pltpu.make_async_remote_copy(
        src_ref=src,
        dst_ref=dst,
        send_sem=send_sem,
        recv_sem=recv_sem,
        device_id={"vp": vp, "dp": dp},
        device_id_type=MESH,
    )


def gather(n, me, dp, own, place, sems, extra, use):
    line = n // 2
    row = me // 2
    side = me - 2 * row
    other = me + 1 - 2 * side
    send_sem, recv_sem = sems

    def copy(way, slot, part, target, src=None):
        src = place(slot, part) if src is None else src
        return send(
            src,
            place(slot, part),
            send_sem.at[way, slot, part],
            recv_sem.at[slot, part],
            target,
            dp,
        )

    for part in range(HALVES):
        copy(0, me, part, other, own(part)).start()

        @pl.when(row < line - 1)
        def _():
            copy(1, me, part, me + 2, own(part)).start()

        @pl.when(row > 0)
        def _():
            copy(2, me, part, me - 2, own(part)).start()

        extra(me, part)
    use(me)

    def crossed(k):
        for part in range(HALVES):
            for step in (-k, k) if k else (0,):
                slot = other + 2 * step

                @pl.when((row + step >= 0) & (row + step < line))
                def _():
                    copy(0, slot, part, other).wait_recv()
                    extra(slot, part)

    def used(k):
        for step in (-k, k) if k else (0,):

            @pl.when((row + step >= 0) & (row + step < line))
            def _():
                use(other + 2 * step)

    for k in range(1, line):
        for part in range(HALVES):
            for step, way in ((-k, 1), (k, 2)):
                slot = me + 2 * step

                @pl.when((row + step >= 0) & (row + step < line))
                def _():
                    copy(0, slot, part, other).wait_recv()
                    on = row < line - 1 if way == 1 else row > 0

                    @pl.when(on)
                    def _():
                        copy(way, slot, part, me + 2 if way == 1 else me - 2).start()

                    copy(0, slot, part, other).start()
                    extra(slot, part)

        crossed(k - 1)
        for step in (-k, k):

            @pl.when((row + step >= 0) & (row + step < line))
            def _():
                use(me + 2 * step)

        used(k - 1)
    crossed(line - 1)
    used(line - 1)

    def finish():
        for part in range(HALVES):
            copy(0, me, part, other, own(part)).wait_send()

            @pl.when(row < line - 1)
            def _():
                copy(1, me, part, me + 2, own(part)).wait_send()

            @pl.when(row > 0)
            def _():
                copy(2, me, part, me - 2, own(part)).wait_send()

            for k in range(1, line):
                for step, way in ((-k, 1), (k, 2)):
                    slot = me + 2 * step

                    @pl.when((row + step >= 0) & (row + step < line))
                    def _():
                        copy(0, slot, part, other).wait_send()

                        @pl.when(row < line - 1 if way == 1 else row > 0)
                        def _():
                            copy(way, slot, part, me).wait_send()

    return finish


def head_kernel(
    n,
    hidden,
    w_down,
    stream,
    gain,
    vocab,
    bias,
    targets,
    loss_out,
    input_out,
    score_out,
    flip_out,
    units,
    stream_cols,
    normin,
    normed,
    words,
    scores,
    tops,
    lanes,
    stats,
    goals,
    total,
    dscore,
    slices,
    terms,
    landed,
    unit_send,
    unit_recv,
    norm_send,
    norm_recv,
    stream_send,
    stream_recv,
    twin_send,
    twin_recv,
    stat_send,
    stat_recv,
    score_send,
    score_recv,
    slice_send,
    slice_recv,
    term_send,
    term_recv,
    load_sem,
    unit_sem,
    out_sem,
):
    me = lax.axis_index("vp")
    dp = lax.axis_index("dp")
    twin = lax.rem(dp + 2, 4)
    core = lax.rem(dp, 2)
    sibling = dp + 1 - 2 * core
    depth, group = hidden.shape
    width = gain.shape[1]
    feats = stream_cols.shape[1]
    rows_dev = stream.shape[0]
    ncols = bias.shape[1]
    own_feats = slices.shape[1]
    half = group // HALVES
    piece = depth // HALVES

    load = pltpu.make_async_copy(vocab, words, load_sem)
    bring = pltpu.make_async_copy(hidden, units.at[me], unit_sem)
    bring.start()
    load.start()
    goals[...] = jnp.transpose(jnp.broadcast_to(targets[...].astype(jnp.float32), (128, group)))
    total[...] = jnp.zeros_like(total)
    barrier = pltpu.get_barrier_semaphore()

    def greet(j, _):
        peer = lax.rem(me + j, n)
        pl.semaphore_signal(barrier, 1, device_id={"vp": peer, "dp": dp}, device_id_type=MESH)
        pl.semaphore_signal(barrier, 1, device_id={"vp": peer, "dp": twin}, device_id_type=MESH)
        return 0

    lax.fori_loop(1, n, greet, 0)
    pl.semaphore_signal(barrier, 1, device_id={"vp": me, "dp": twin}, device_id_type=MESH)
    pl.semaphore_signal(barrier, 1, device_id={"vp": me, "dp": sibling}, device_id_type=MESH)
    pl.semaphore_wait(barrier, 2 * n)

    def stream_copy(j):
        peer = lax.rem(me + j, n)
        return send(
            stream.at[:, pl.ds(pl.multiple_of(peer * feats, 128), feats)],
            stream_cols.at[pl.ds(pl.multiple_of(me * rows_dev, rows_dev), rows_dev), :],
            stream_send.at[j],
            stream_recv.at[j],
            peer,
            dp,
        )

    def start_stream(j, _):
        stream_copy(j).start()
        return 0

    def wait_stream(j, _):
        stream_copy(j).wait()
        return 0

    bring.wait()
    stream_cols[pl.ds(pl.multiple_of(me * rows_dev, rows_dev), rows_dev), :] = stream[
        :, pl.ds(pl.multiple_of(me * feats, 128), feats)
    ]
    lax.fori_loop(1, n, start_stream, 0)
    def place_units(slot, part):
        return units.at[slot, pl.ds(part * piece, piece), :]

    def project(slot):
        rows = pl.ds(pl.multiple_of(slot * depth, 16), depth)
        total[...] += lax.dot_general(
            units[slot],
            w_down[rows, :],
            (((0,), (0,)), ((), ())),
            preferred_element_type=jnp.float32,
        )

    finish_units = gather(
        n,
        me,
        dp,
        lambda part: place_units(me, part),
        place_units,
        (unit_send, unit_recv),
        lambda slot, part: None,
        project,
    )
    lax.fori_loop(1, n, wait_stream, 0)

    def cols_of(slot):
        return pl.ds(pl.multiple_of(slot * feats, 128), feats)

    normin[0, :, cols_of(me)] = (stream_cols[...].astype(jnp.float32) + total[...]).astype(jnp.bfloat16)

    def twin_copy(slot, part):
        rows = pl.ds(part * half, half)
        return send(
            normin.at[0, rows, cols_of(slot)],
            normin.at[1, rows, cols_of(slot)],
            twin_send.at[slot, part],
            twin_recv.at[slot, part],
            me,
            twin,
        )

    finish_norm = gather(
        n,
        me,
        dp,
        lambda part: normin.at[0, pl.ds(part * half, half), cols_of(me)],
        lambda slot, part: normin.at[0, pl.ds(part * half, half), cols_of(slot)],
        (norm_send, norm_recv),
        lambda slot, part: twin_copy(slot, part).start(),
        lambda slot: None,
    )

    def normalize(which):
        def block(j, _):
            rows = pl.ds(pl.multiple_of(j * 32, 32), 32)
            values = normin[which, rows, :].astype(jnp.float32)
            inv = lax.rsqrt(jnp.mean(values * values, axis=1, keepdims=True) + norm_eps)
            normed[which, rows, :] = (values * inv * gain[...]).astype(jnp.bfloat16)
            return 0

        lax.fori_loop(0, group // 32, block, 0)

    def slice_copy(which, home):
        rows = pl.ds(pl.multiple_of(home * group, group), group)
        cols = pl.ds(pl.multiple_of(sibling * own_feats, 128), own_feats)
        return send(
            normed.at[which, :, cols],
            slices.at[rows, :],
            slice_send.at[which],
            slice_recv.at[which],
            me,
            sibling,
        )

    def folded(values, join):
        result = values[:, :128]
        for at in range(128, TILE, 128):
            result = join(result, values[:, at : at + 128])
        return result

    def score(which, first, last):
        def block(j, _):
            cols = pl.ds(pl.multiple_of(j * TILE, TILE), TILE)
            values = (
                jnp.dot(normed[which], words[:, cols], preferred_element_type=jnp.float32)
                + bias[:, cols]
            )
            scores[which, :, cols] = values
            tops[which] = jnp.maximum(tops[which], folded(values, jnp.maximum))
            return 0

        lax.fori_loop(first, last, block, 0)

    def level(which):
        top = jnp.max(tops[which], axis=1, keepdims=True)
        tops[which] = jnp.broadcast_to(top, (group, 128))
        lanes[...] = jnp.zeros_like(lanes)

        def powers(j, _):
            cols = pl.ds(pl.multiple_of(j * TILE, TILE), TILE)
            values = scores[which, :, cols]
            if which == 0:
                ids = lax.broadcasted_iota(jnp.int32, (group, TILE), 1) + (me * ncols + j * TILE)
                hits = jnp.where(ids == own_goals, values, 0.0)
                lanes[1] += folded(hits, jnp.add)
            values = jnp.exp(values - top)
            scores[which, :, cols] = values
            if which == 0:
                lanes[0] += folded(values, jnp.add)
            return 0

        lax.fori_loop(0, ncols // TILE, powers, 0)
        return top

    def stat_copy(away, j, home):
        peer = lax.rem(me + j, n)
        return send(
            stats.at[0, me],
            stats.at[away, me],
            stat_send.at[away, j],
            stat_recv.at[away, j],
            peer,
            home,
        )

    tops[...] = jnp.full(tops.shape, -jnp.inf, jnp.float32)
    own_goals = goals[:, 0:1].astype(jnp.int32)
    blocks = ncols // TILE
    middle = blocks // 2
    normalize(0)
    load.wait()
    slice_copy(0, dp).start()
    score(0, 0, blocks)
    top = level(0)
    lane = lax.broadcasted_iota(jnp.int32, (group, 128), 1)
    packed = jnp.where(
        lane == 0,
        top,
        jnp.where(
            lane == 1,
            jnp.sum(lanes[0], axis=1, keepdims=True),
            jnp.where(
                lane == 2,
                jnp.sum(lanes[1], axis=1, keepdims=True),
                jnp.where(lane == 3, goals[...], 0.0),
            ),
        ),
    )
    stats[0, me] = jnp.transpose(packed)[:8, :]

    def start_stats(j, _):
        stat_copy(0, j, dp).start()
        stat_copy(1, j, twin).start()
        return 0

    stat_copy(1, 0, twin).start()
    lax.fori_loop(1, n, start_stats, 0)

    for slot in range(n):
        for part in range(HALVES):
            twin_copy(slot, part).wait()
    normalize(1)
    slice_copy(1, twin).start()
    score(1, 0, middle)

    def wait_stats(away, home):
        def wait(j, _):
            stat_copy(away, j, home).wait()
            return 0

        lax.fori_loop(1, n, wait, 0)

    def score_copy(which, home):
        rows = pl.ds(pl.multiple_of(home * group, group), group)
        return send(
            dscore.at[which],
            score_out.at[rows, :],
            score_send.at[which],
            score_recv.at[which],
            me,
            sibling,
        )

    def keep_copy(which, home):
        rows = pl.ds(pl.multiple_of(home * group, group), group)
        return pltpu.make_async_copy(dscore.at[which], score_out.at[rows, :], out_sem.at[which])

    def derive(which, home):
        parts = stats[which]
        highest = jnp.max(parts[:, 0, :], axis=0, keepdims=True)
        total = jnp.sum(parts[:, 1, :] * jnp.exp(parts[:, 0, :] - highest), axis=0, keepdims=True)
        lse = highest + jnp.log(total)
        if which == 0:
            goal = jnp.sum(parts[:, 2, :], axis=0, keepdims=True)
            loss_out[...] = jnp.broadcast_to(lse - goal + zloss_weight * lse * lse, (8, group))
        line = lax.broadcasted_iota(jnp.int32, (128, group), 0)
        turned = jnp.transpose(
            jnp.where(line == 0, lse, jnp.where(line == 1, parts[0, 3:4, :], 0.0))
        )
        lse_col = turned[:, 0:1]
        goal_col = turned[:, 1:2].astype(jnp.int32)
        factor = jnp.exp(tops[which][:, 0:1] - lse_col) * (1.0 + 2.0 * zloss_weight * lse_col)

        def block(j, _):
            cols = pl.ds(pl.multiple_of(j * TILE, TILE), TILE)
            ids = lax.broadcasted_iota(jnp.int32, (group, TILE), 1) + (me * ncols + j * TILE)
            values = scores[which, :, cols] * factor - jnp.where(ids == goal_col, 1.0, 0.0)
            dscore[which, :, cols] = values.astype(jnp.bfloat16)
            return 0

        lax.fori_loop(0, ncols // TILE, block, 0)
        score_copy(which, home).start()
        keep_copy(which, home).start()

    wait_stats(0, dp)
    derive(0, dp)

    def term_copy(t, j):
        peer = lax.rem(me + j, n)
        cols = pl.ds(pl.multiple_of(t * TILE, TILE), TILE)
        return send(
            terms.at[pl.ds(pl.multiple_of(peer * rows_dev, rows_dev), rows_dev), cols],
            landed.at[me, :, cols],
            term_send.at[t, j],
            term_recv.at[t, j],
            peer,
            dp,
        )

    def term_block(t, _):
        cols = pl.ds(pl.multiple_of(t * TILE, TILE), TILE)
        terms[:, cols] = lax.dot_general(
            dscore[0],
            words[cols, :],
            (((1,), (1,)), ((), ())),
            preferred_element_type=jnp.float32,
        ).astype(jnp.bfloat16)

        def start(j, _):
            term_copy(t, j).start()
            return 0

        return lax.fori_loop(1, n, start, 0)

    lax.fori_loop(0, width // TILE, term_block, 0)
    my_rows = pl.ds(pl.multiple_of(me * rows_dev, rows_dev), rows_dev)
    landed[me] = terms[my_rows, :]
    score(1, middle, blocks)
    level(1)
    stat_copy(1, 0, twin).wait()
    wait_stats(1, twin)
    derive(1, twin)

    for which, home in ((0, dp), (1, twin)):
        rows = pl.ds(pl.multiple_of(home * group, group), group)
        slices[rows, :] = normed[which, :, pl.ds(pl.multiple_of(dp * own_feats, 128), own_feats)]
        slice_copy(which, home).wait()
    flip_out[...] = jnp.transpose(slices[...])

    def wait_terms(t, _):
        def wait(j, _):
            term_copy(t, j).wait()
            return 0

        return lax.fori_loop(1, n, wait, 0)

    lax.fori_loop(0, width // TILE, wait_terms, 0)
    values = normin[0, my_rows, :].astype(jnp.float32)
    inv = lax.rsqrt(jnp.mean(values * values, axis=1, keepdims=True) + norm_eps)
    dnormed = landed[0].astype(jnp.float32)
    for slot in range(1, n):
        dnormed += landed[slot].astype(jnp.float32)
    scaled = dnormed * gain[...]
    input_out[...] = inv * (
        scaled - values * inv * inv * jnp.mean(values * scaled, axis=1, keepdims=True)
    )
    for which, home in ((0, dp), (1, twin)):
        keep_copy(which, home).wait()
        score_copy(which, home).wait()
    finish_units()
    finish_norm()


def vocab_kernel(flipped, dscore, grad_input, losses, vocab_out, input_out, loss_out):
    rows_dev = loss_out.shape[1]
    group = losses.shape[1]
    vocab_out[...] = jnp.dot(flipped[...], dscore[...], preferred_element_type=jnp.float32)

    @pl.when(pl.program_id(0) == 0)
    def _():
        input_out[...] = grad_input[...]
        shift = lax.rem(group - lax.axis_index("vp") * rows_dev, group)
        loss_out[...] = pltpu.roll(losses[...], shift, 1)[0:1, :rows_dev]


def fused(stream, hidden, w_down, final_gain, vocab, vocab_bias, targets):
    n = lax.axis_size("vp")
    groups = lax.axis_size("dp")
    rows_dev, width = stream.shape
    group, depth = hidden.shape
    feats = w_down.shape[1]
    ncols = vocab.shape[1]
    own_feats = width // groups
    tokens = groups * group
    f32, bf16 = jnp.float32, jnp.bfloat16
    dma = pltpu.SemaphoreType.DMA
    vmem = pl.BlockSpec(memory_space=pltpu.VMEM)
    hbm = pl.BlockSpec(memory_space=pl.ANY)
    group_losses, grad_input, dscore, flipped = pl.pallas_call(
        functools.partial(head_kernel, n),
        out_shape=(
            jax.ShapeDtypeStruct((8, group), f32),
            jax.ShapeDtypeStruct((rows_dev, width), f32),
            jax.ShapeDtypeStruct((tokens, ncols), bf16),
            jax.ShapeDtypeStruct((own_feats, tokens), bf16),
        ),
        in_specs=[hbm, vmem, vmem, vmem, hbm, vmem, vmem],
        out_specs=(vmem, vmem, hbm, vmem),
        scratch_shapes=[
            pltpu.VMEM((n, depth, group), bf16),
            pltpu.VMEM((group, feats), bf16),
            pltpu.VMEM((2, group, width), bf16),
            pltpu.VMEM((2, group, width), bf16),
            pltpu.VMEM((width, ncols), bf16),
            pltpu.VMEM((2, group, ncols), f32),
            pltpu.VMEM((2, group, 128), f32),
            pltpu.VMEM((2, group, 128), f32),
            pltpu.VMEM((2, n, 8, group), f32),
            pltpu.VMEM((group, 128), f32),
            pltpu.VMEM((group, feats), f32),
            pltpu.VMEM((2, group, ncols), bf16),
            pltpu.VMEM((tokens, own_feats), bf16),
            pltpu.VMEM((group, width), bf16),
            pltpu.VMEM((n, rows_dev, width), bf16),
            dma((3, n, HALVES)),
            dma((n, HALVES)),
            dma((3, n, HALVES)),
            dma((n, HALVES)),
            dma((n,)),
            dma((n,)),
            dma((n, HALVES)),
            dma((n, HALVES)),
            dma((2, n)),
            dma((2, n)),
            dma((2,)),
            dma((2,)),
            dma((2,)),
            dma((2,)),
            dma((width // TILE, n)),
            dma((width // TILE, n)),
            dma,
            dma,
            dma((2,)),
        ],
        compiler_params=pltpu.CompilerParams(
            collective_id=0, has_side_effects=True, vmem_limit_bytes=64 * 1024 * 1024 - 65536
        ),
    )(
        hidden.T,
        w_down,
        stream,
        final_gain.reshape(1, width),
        vocab,
        vocab_bias.reshape(1, ncols),
        targets.reshape(1, group),
    )

    def whole(*shape):
        return pl.BlockSpec(shape, lambda j: (0, 0))

    grad_vocab, grad_input, losses = pl.pallas_call(
        vocab_kernel,
        grid=(ncols // TILE,),
        out_shape=(
            jax.ShapeDtypeStruct((own_feats, ncols), f32),
            jax.ShapeDtypeStruct((rows_dev, width), f32),
            jax.ShapeDtypeStruct((1, rows_dev), f32),
        ),
        in_specs=[
            whole(own_feats, tokens),
            pl.BlockSpec((tokens, TILE), lambda j: (0, j)),
            whole(rows_dev, width),
            whole(8, group),
        ],
        out_specs=(
            pl.BlockSpec((own_feats, TILE), lambda j: (0, j)),
            whole(rows_dev, width),
            whole(1, rows_dev),
        ),
    )(flipped, dscore, grad_input, group_losses)
    return (losses.reshape(rows_dev), grad_input, grad_vocab)


def choose(stream, hidden, w_down, final_gain, vocab, vocab_bias, targets):
    rows_dev, width = stream.shape
    group, depth = hidden.shape
    n, groups = lax.axis_size("vp"), lax.axis_size("dp")
    tiles = (
        n % 2 == 0
        and groups == 4
        and rows_dev % 32 == 0
        and depth % (16 * HALVES) == 0
        and group % (32 * HALVES) == 0
        and w_down.shape[1] % 128 == 0
        and width % TILE == 0
        and (width // groups) % 128 == 0
        and vocab.shape[1] % TILE == 0
    )
    path = fused if tiles else body
    return path(stream, hidden, w_down, final_gain, vocab, vocab_bias, targets)


def solution(mesh):
    placed = (
        P(("dp", "vp"), None),
        P("dp", "vp"),
        P(None, "vp"),
        P(),
        P(None, "vp"),
        P("vp"),
        P("dp"),
    )
    return jax.shard_map(
        choose,
        mesh=mesh,
        in_specs=placed,
        out_specs=(P(("dp", "vp")), P(("dp", "vp"), None), P("dp", "vp")),
        check_vma=False,
    )
```

profile of v0, /device:TPU:0, one launch (start us, length us, event | category | flops | bytes accessed | tf_op | source)
XLA Modules:
  0.0 110.4 jit_solution(112721965959320709)
XLA Ops:
  0.6 98.4 %shard_map.94 = (f32[8,256]{1,0:T(8,128)}, f32[32,2048]{1,0:T(8,128)}, bf16[1024,4096]{1,0:T(8,128)(2,1)}, bf16[512,1024]{1,0:T(8,128)(2,1)}) custom-call(bf16[704,256]{1,0:T(8,128)(2,1)} %bitcast.5, bf16[5632,256]{1,0:T(8,128)(2,1)} %w_down.1, bf16[32,2048]{1,0:T(8,128)(2,1)} %stream.1, f32[1,2048]{1,0:T(1,128)} %bitcast.7, bf16[2048,4096]{1,0:T(8,128)(2,1)} %vocab.1, ...), custom_call_target="tpu_custom_call" | custom-call | tf_op jit(solution)/shard_map/pallas_call | solution.py:622
  99.1 11.3 %shard_map.95 = (f32[512,4096]{1,0:T(8,128)}, f32[32,2048]{1,0:T(8,128)}, f32[1,32]{1,0:T(1,128)}) custom-call(bf16[512,1024]{1,0:T(8,128)(2,1)} %get-tuple-element.10.flipped, bf16[1024,4096]{1,0:T(8,128)(2,1)} %get-tuple-element.11.dscore, f32[32,2048]{1,0:T(8,128)} %get-tuple-element.12.grad_input, f32[8,256]{1,0:T(8,128)} %get-tuple-element.13.losses), custom_call_target="tpu_custom_call" | custom-call | tf_op jit(solution)/shard_map/pallas_call | solution.py:684
where the time goes:
time: 111 us; the launch traced here: 110 us
  Pallas kernels  110 us (99%)
    pallas_call x1, Pallas kernels, fused(): pl.pallas_call(functools.partial(head_kernel, n), out_shape=(jax.ShapeDty...  98.4 us
    pallas_call x1, Pallas kernels, fused(): pl.pallas_call(vocab_kernel, grid=(ncols // TILE,), out_shape=(jax.ShapeD...  11.3 us

commit v1 on v0

--- a/solution.py
+++ b/solution.py
@@ -88,8 +88,10 @@
 
 
 MESH = pl.DeviceIdType.MESH
-HALVES = 2
+UNIT_PARTS = 2
+NORM_PARTS = 4
 TILE = 512
+BLOCK = 512
 
 
 def send(src, dst, send_sem, recv_sem, vp, dp):
@@ -103,123 +105,154 @@
     )
 
 
-def gather(n, me, dp, own, place, sems, extra, use):
+def gather(n, me, dp, parts, own, place, bulk, sems, extra, first, use):
     line = n // 2
-    row = me // 2
-    side = me - 2 * row
+    here = me // 2
+    side = me - 2 * here
     other = me + 1 - 2 * side
+    turn = parts // 2
     send_sem, recv_sem = sems
-
-    def copy(way, slot, part, target, src=None):
-        src = place(slot, part) if src is None else src
+    targets = {0: other, 1: me + 2, 2: me - 2}
+    sent = []
+
+    def copy(way, slot, part, src=None):
         return send(
-            src,
+            place(slot, part) if src is None else src,
             place(slot, part),
-            send_sem.at[way, slot, part],
+            send_sem.at[way],
             recv_sem.at[slot, part],
-            target,
+            targets[way],
             dp,
         )
 
-    for part in range(HALVES):
-        copy(0, me, part, other, own(part)).start()
-
-        @pl.when(row < line - 1)
-        def _():
-            copy(1, me, part, me + 2, own(part)).start()
-
-        @pl.when(row > 0)
-        def _():
-            copy(2, me, part, me - 2, own(part)).start()
-
+    def holds(conditions, row):
+        return functools.reduce(lambda a, b: a & b, [test(row) for test in conditions])
+
+    def when(conditions, action):
+        if conditions:
+            pl.when(holds(conditions, here))(action)
+        else:
+            action()
+
+    def put(outer, inner, way, slot, part, src=None):
+        when(inner, lambda: copy(way, slot, part, src).start())
+        sent.append((outer + inner, way))
+
+    def live(step):
+        if step == 0:
+            return []
+        return [lambda row: (row + step < line) & (row + step >= 0)]
+
+    def ends(step):
+        return [lambda row: row + step == (line - 1 if step > 0 else 0)]
+
+    def inside(step):
+        return [lambda row: row + step != (line - 1 if step > 0 else 0)]
+
+    up, down = [lambda row: row < line - 1], [lambda row: row > 0]
+
+    for part in range(parts):
+        put([], [], 0, me, part, own(part))
+        put([], up, 1, me, part, own(part))
+        put([], down, 2, me, part, own(part))
         extra(me, part)
-    use(me)
+    first()
+
+    def straight(k, part, step, way):
+        slot = me + 2 * step
+        outer = live(step)
+
+        def receive():
+            copy(0, slot, part).wait_recv()
+            put(outer, up if way == 1 else down, way, slot, part)
+            put(outer, inside(step) if part >= turn else [], 0, slot, part)
+            extra(slot, part)
+
+        when(outer, receive)
+
+    def routed(k):
+        for step, way in ((-k, 1), (k, 2)):
+            slot = other + 2 * step
+            outer = live(step) + ends(step)
+
+            def receive(slot=slot, outer=outer, way=way):
+                for part in range(turn, parts):
+                    copy(0, slot, part).wait_recv()
+                    put(outer, up if way == 1 else down, way, slot, part)
+                    extra(slot, part)
+
+            when(outer, receive)
 
     def crossed(k):
-        for part in range(HALVES):
+        for part in range(parts):
             for step in (-k, k) if k else (0,):
                 slot = other + 2 * step
-
-                @pl.when((row + step >= 0) & (row + step < line))
-                def _():
-                    copy(0, slot, part, other).wait_recv()
+                outer = live(step)
+                if k and part >= turn:
+                    outer = outer + inside(step)
+
+                def receive(slot=slot, part=part):
+                    copy(0, slot, part).wait_recv()
                     extra(slot, part)
 
-    def used(k):
+                when(outer, receive)
+                if k == 0 and part >= turn:
+                    put([], [lambda row: row == 0] + up, 1, slot, part)
+                    put([], [lambda row: row == line - 1] + down, 2, slot, part)
+
+    def used(base, k):
         for step in (-k, k) if k else (0,):
-
-            @pl.when((row + step >= 0) & (row + step < line))
-            def _():
-                use(other + 2 * step)
+            when(live(step), lambda step=step: use(base + 2 * step))
 
     for k in range(1, line):
-        for part in range(HALVES):
-            for step, way in ((-k, 1), (k, 2)):
-                slot = me + 2 * step
-
-                @pl.when((row + step >= 0) & (row + step < line))
-                def _():
-                    copy(0, slot, part, other).wait_recv()
-                    on = row < line - 1 if way == 1 else row > 0
-
-                    @pl.when(on)
-                    def _():
-                        copy(way, slot, part, me + 2 if way == 1 else me - 2).start()
-
-                    copy(0, slot, part, other).start()
-                    extra(slot, part)
-
+        for part in range(parts):
+            straight(k, part, -k, 1)
+            straight(k, part, k, 2)
+        if k > 1:
+            routed(k - 1)
         crossed(k - 1)
-        for step in (-k, k):
-
-            @pl.when((row + step >= 0) & (row + step < line))
-            def _():
-                use(me + 2 * step)
-
-        used(k - 1)
+        used(me, k)
+        used(other, k - 1)
+    if line > 1:
+        routed(line - 1)
     crossed(line - 1)
-    used(line - 1)
+    used(other, line - 1)
 
     def finish():
-        for part in range(HALVES):
-            copy(0, me, part, other, own(part)).wait_send()
-
-            @pl.when(row < line - 1)
-            def _():
-                copy(1, me, part, me + 2, own(part)).wait_send()
-
-            @pl.when(row > 0)
-            def _():
-                copy(2, me, part, me - 2, own(part)).wait_send()
-
-            for k in range(1, line):
-                for step, way in ((-k, 1), (k, 2)):
-                    slot = me + 2 * step
-
-                    @pl.when((row + step >= 0) & (row + step < line))
-                    def _():
-                        copy(0, slot, part, other).wait_send()
-
-                        @pl.when(row < line - 1 if way == 1 else row > 0)
-                        def _():
-                            copy(way, slot, part, me).wait_send()
+        for way in range(3):
+            for row in range(line):
+                count = sum(1 for tests, which in sent if which == way and (not tests or holds(tests, row)))
+                if count:
+                    pl.when(here == row)(lambda: await_bytes(bulk(count), send_sem.at[way]))
 
     return finish
+
+
+def await_bytes(ref, sem):
+    pltpu.make_async_copy(ref, ref, sem).wait()
 
 
 def head_kernel(
     n,
     hidden,
-    w_down,
-    stream,
-    gain,
+    w_down_in,
+    stream_in,
+    gain_in,
     vocab,
-    bias,
-    targets,
+    bias_in,
+    targets_in,
     loss_out,
     input_out,
     score_out,
     flip_out,
+    w_down,
+    stream,
+    gain,
+    bias,
+    targets,
+    loss_buf,
+    input_buf,
+    flip_buf,
     units,
     stream_cols,
     normin,
@@ -234,6 +267,8 @@
     dscore,
     slices,
     terms,
+    crossing,
+    sums,
     landed,
     unit_send,
     unit_recv,
@@ -249,10 +284,12 @@
     score_recv,
     slice_send,
     slice_recv,
+    cross_send,
+    cross_recv,
     term_send,
     term_recv,
     load_sem,
-    unit_sem,
+    keep_sem,
     out_sem,
 ):
     me = lax.axis_index("vp")
@@ -260,21 +297,19 @@
     twin = lax.rem(dp + 2, 4)
     core = lax.rem(dp, 2)
     sibling = dp + 1 - 2 * core
+    line = n // 2
+    place = me // 2
+    side = me - 2 * place
+    other = me + 1 - 2 * side
     depth, group = hidden.shape
     width = gain.shape[1]
     feats = stream_cols.shape[1]
     rows_dev = stream.shape[0]
     ncols = bias.shape[1]
     own_feats = slices.shape[1]
-    half = group // HALVES
-    piece = depth // HALVES
-
-    load = pltpu.make_async_copy(vocab, words, load_sem)
-    bring = pltpu.make_async_copy(hidden, units.at[me], unit_sem)
-    bring.start()
-    load.start()
-    goals[...] = jnp.transpose(jnp.broadcast_to(targets[...].astype(jnp.float32), (128, group)))
-    total[...] = jnp.zeros_like(total)
+    half = group // NORM_PARTS
+    piece = depth // UNIT_PARTS
+
     barrier = pltpu.get_barrier_semaphore()
 
     def greet(j, _):
@@ -286,6 +321,19 @@
     lax.fori_loop(1, n, greet, 0)
     pl.semaphore_signal(barrier, 1, device_id={"vp": me, "dp": twin}, device_id_type=MESH)
     pl.semaphore_signal(barrier, 1, device_id={"vp": me, "dp": sibling}, device_id_type=MESH)
+
+    def brought(at, src, dst):
+        return pltpu.make_async_copy(src, dst, load_sem.at[at])
+
+    bring = brought(0, hidden, units.at[pl.ds(pl.multiple_of(me * depth, 16), depth), :])
+    bring_stream = brought(1, stream_in, stream)
+    bring_down = brought(2, w_down_in, w_down)
+    bring_targets = brought(3, targets_in, targets)
+    bring_gain = brought(4, gain_in, gain)
+    bring_bias = brought(5, bias_in, bias)
+    load = brought(6, vocab, words)
+    for copy in (bring, bring_stream, bring_down, bring_targets, bring_gain, bring_bias, load):
+        copy.start()
     pl.semaphore_wait(barrier, 2 * n)
 
     def stream_copy(j):
@@ -293,8 +341,8 @@
         return send(
             stream.at[:, pl.ds(pl.multiple_of(peer * feats, 128), feats)],
             stream_cols.at[pl.ds(pl.multiple_of(me * rows_dev, rows_dev), rows_dev), :],
-            stream_send.at[j],
-            stream_recv.at[j],
+            stream_send,
+            stream_recv,
             peer,
             dp,
         )
@@ -303,38 +351,51 @@
         stream_copy(j).start()
         return 0
 
-    def wait_stream(j, _):
-        stream_copy(j).wait()
-        return 0
-
-    bring.wait()
-    stream_cols[pl.ds(pl.multiple_of(me * rows_dev, rows_dev), rows_dev), :] = stream[
-        :, pl.ds(pl.multiple_of(me * feats, 128), feats)
-    ]
-    lax.fori_loop(1, n, start_stream, 0)
     def place_units(slot, part):
-        return units.at[slot, pl.ds(part * piece, piece), :]
-
-    def project(slot):
+        return units.at[pl.ds(pl.multiple_of(slot * depth + part * piece, 16), piece), :]
+
+    def product(slot):
         rows = pl.ds(pl.multiple_of(slot * depth, 16), depth)
-        total[...] += lax.dot_general(
-            units[slot],
+        return lax.dot_general(
+            units[rows, :],
             w_down[rows, :],
             (((0,), (0,)), ((), ())),
             preferred_element_type=jnp.float32,
         )
 
+    def open_units():
+        bring_stream.wait()
+        lax.fori_loop(1, n, start_stream, 0)
+        stream_cols[pl.ds(pl.multiple_of(me * rows_dev, rows_dev), rows_dev), :] = stream[
+            :, pl.ds(pl.multiple_of(me * feats, 128), feats)
+        ]
+        bring_targets.wait()
+        goals[...] = jnp.transpose(
+            jnp.broadcast_to(targets[...].astype(jnp.float32), (128, group))
+        )
+        bring_down.wait()
+        total[...] = product(me)
+
+    def project(slot):
+        total[...] += product(slot)
+
+    bring.wait()
     finish_units = gather(
         n,
         me,
         dp,
+        UNIT_PARTS,
         lambda part: place_units(me, part),
         place_units,
+        lambda count: units.at[pl.ds(0, count * piece), :],
         (unit_send, unit_recv),
         lambda slot, part: None,
+        open_units,
         project,
     )
-    lax.fori_loop(1, n, wait_stream, 0)
+    streamed = stream_cols.at[pl.ds(0, (n - 1) * rows_dev), :]
+    await_bytes(streamed, stream_recv)
+    await_bytes(streamed, stream_send)
 
     def cols_of(slot):
         return pl.ds(pl.multiple_of(slot * feats, 128), feats)
@@ -346,20 +407,31 @@
         return send(
             normin.at[0, rows, cols_of(slot)],
             normin.at[1, rows, cols_of(slot)],
-            twin_send.at[slot, part],
-            twin_recv.at[slot, part],
+            twin_send,
+            twin_recv,
             me,
             twin,
         )
+
+    def place_norm(slot, part):
+        return normin.at[0, pl.ds(part * half, half), cols_of(slot)]
+
+    def open_norm():
+        bring_gain.wait()
+        bring_bias.wait()
+        tops[...] = jnp.full(tops.shape, -jnp.inf, jnp.float32)
 
     finish_norm = gather(
         n,
         me,
         dp,
-        lambda part: normin.at[0, pl.ds(part * half, half), cols_of(me)],
-        lambda slot, part: normin.at[0, pl.ds(part * half, half), cols_of(slot)],
+        NORM_PARTS,
+        lambda part: place_norm(me, part),
+        place_norm,
+        lambda count: scores.at[0, pl.ds(0, count * half // 8), pl.ds(0, 4 * feats)],
         (norm_send, norm_recv),
         lambda slot, part: twin_copy(slot, part).start(),
+        open_norm,
         lambda slot: None,
     )
 
@@ -430,16 +502,14 @@
         return send(
             stats.at[0, me],
             stats.at[away, me],
-            stat_send.at[away, j],
-            stat_recv.at[away, j],
+            stat_send.at[away],
+            stat_recv.at[away],
             peer,
             home,
         )
 
-    tops[...] = jnp.full(tops.shape, -jnp.inf, jnp.float32)
     own_goals = goals[:, 0:1].astype(jnp.int32)
     blocks = ncols // TILE
-    middle = blocks // 2
     normalize(0)
     load.wait()
     slice_copy(0, dp).start()
@@ -463,40 +533,42 @@
 
     def start_stats(j, _):
         stat_copy(0, j, dp).start()
+        return 0
+
+    def start_away(j, _):
         stat_copy(1, j, twin).start()
         return 0
 
-    stat_copy(1, 0, twin).start()
     lax.fori_loop(1, n, start_stats, 0)
-
-    for slot in range(n):
-        for part in range(HALVES):
-            twin_copy(slot, part).wait()
-    normalize(1)
-    slice_copy(1, twin).start()
-    score(1, 0, middle)
-
-    def wait_stats(away, home):
-        def wait(j, _):
-            stat_copy(away, j, home).wait()
-            return 0
-
-        lax.fori_loop(1, n, wait, 0)
-
-    def score_copy(which, home):
+    lax.fori_loop(0, n, start_away, 0)
+
+    def wait_stats(away):
+        arrived = stats.at[away, pl.ds(0, n - 1 + away)]
+        await_bytes(arrived, stat_recv.at[away])
+        await_bytes(arrived, stat_send.at[away])
+
+    def score_copy(which, home, j):
         rows = pl.ds(pl.multiple_of(home * group, group), group)
+        cols = pl.ds(pl.multiple_of(j * TILE, TILE), TILE)
         return send(
-            dscore.at[which],
-            score_out.at[rows, :],
+            dscore.at[which, :, cols],
+            score_out.at[rows, cols],
             score_send.at[which],
             score_recv.at[which],
             me,
             sibling,
         )
 
-    def keep_copy(which, home):
+    def keep_copy(which, home, j):
         rows = pl.ds(pl.multiple_of(home * group, group), group)
-        return pltpu.make_async_copy(dscore.at[which], score_out.at[rows, :], out_sem.at[which])
+        cols = pl.ds(pl.multiple_of(j * TILE, TILE), TILE)
+        return pltpu.make_async_copy(
+            dscore.at[which, :, cols], score_out.at[rows, cols], keep_sem.at[which]
+        )
+
+    loss_copy = pltpu.make_async_copy(loss_buf, loss_out, out_sem.at[0])
+    flip_copy = pltpu.make_async_copy(flip_buf, flip_out, out_sem.at[1])
+    input_copy = pltpu.make_async_copy(input_buf, input_out, out_sem.at[2])
 
     def derive(which, home):
         parts = stats[which]
@@ -505,10 +577,11 @@
         lse = highest + jnp.log(total)
         if which == 0:
             goal = jnp.sum(parts[:, 2, :], axis=0, keepdims=True)
-            loss_out[...] = jnp.broadcast_to(lse - goal + zloss_weight * lse * lse, (8, group))
-        line = lax.broadcasted_iota(jnp.int32, (128, group), 0)
+            loss_buf[...] = jnp.broadcast_to(lse - goal + zloss_weight * lse * lse, (8, group))
+            loss_copy.start()
+        column = lax.broadcasted_iota(jnp.int32, (128, group), 0)
         turned = jnp.transpose(
-            jnp.where(line == 0, lse, jnp.where(line == 1, parts[0, 3:4, :], 0.0))
+            jnp.where(column == 0, lse, jnp.where(column == 1, parts[0, 3:4, :], 0.0))
         )
         lse_col = turned[:, 0:1]
         goal_col = turned[:, 1:2].astype(jnp.int32)
@@ -519,91 +592,176 @@
             ids = lax.broadcasted_iota(jnp.int32, (group, TILE), 1) + (me * ncols + j * TILE)
             values = scores[which, :, cols] * factor - jnp.where(ids == goal_col, 1.0, 0.0)
             dscore[which, :, cols] = values.astype(jnp.bfloat16)
+            score_copy(which, home, j).start()
+            keep_copy(which, home, j).start()
             return 0
 
         lax.fori_loop(0, ncols // TILE, block, 0)
-        score_copy(which, home).start()
-        keep_copy(which, home).start()
-
-    wait_stats(0, dp)
+
+    wait_stats(0)
     derive(0, dp)
 
-    def term_copy(t, j):
-        peer = lax.rem(me + j, n)
+    def cross_copy(t):
         cols = pl.ds(pl.multiple_of(t * TILE, TILE), TILE)
         return send(
-            terms.at[pl.ds(pl.multiple_of(peer * rows_dev, rows_dev), rows_dev), cols],
-            landed.at[me, :, cols],
-            term_send.at[t, j],
-            term_recv.at[t, j],
-            peer,
+            terms.at[:, 1 - side, :, cols],
+            crossing.at[:, :, cols],
+            cross_send,
+            cross_recv.at[t],
+            other,
+            dp,
+        )
+
+    def term_copy(t, j):
+        peer = lax.rem(place + j, line)
+        cols = pl.ds(pl.multiple_of(t * TILE, TILE), TILE)
+        return send(
+            sums.at[peer, :, cols],
+            landed.at[place, :, cols],
+            term_send,
+            term_recv,
+            2 * peer + side,
             dp,
         )
 
     def term_block(t, _):
         cols = pl.ds(pl.multiple_of(t * TILE, TILE), TILE)
-        terms[:, cols] = lax.dot_general(
+        block = lax.dot_general(
             dscore[0],
             words[cols, :],
             (((1,), (1,)), ((), ())),
             preferred_element_type=jnp.float32,
         ).astype(jnp.bfloat16)
-
-        def start(j, _):
+        terms[:, :, :, cols] = block.reshape(line, 2, rows_dev, TILE)
+        cross_copy(t).start()
+        return 0
+
+    def pass_on(t):
+        cols = pl.ds(t * TILE, TILE)
+        cross_copy(t).wait_recv()
+        both = terms[:, side, :, cols].astype(jnp.float32) + crossing[:, :, cols].astype(jnp.float32)
+        sums[:, :, cols] = both.astype(jnp.bfloat16)
+        for j in range(1, line):
             term_copy(t, j).start()
-            return 0
-
-        return lax.fori_loop(1, n, start, 0)
+        landed[place, :, cols] = sums[place, :, cols]
 
     lax.fori_loop(0, width // TILE, term_block, 0)
-    my_rows = pl.ds(pl.multiple_of(me * rows_dev, rows_dev), rows_dev)
-    landed[me] = terms[my_rows, :]
-    score(1, middle, blocks)
-    level(1)
-    stat_copy(1, 0, twin).wait()
-    wait_stats(1, twin)
-    derive(1, twin)
-
+    await_bytes(normin.at[1], twin_recv)
+    await_bytes(normin.at[1], twin_send)
+    normalize(1)
+    slice_copy(1, twin).start()
+    tiles = width // TILE
+    done = 0
+    for t in range(tiles):
+        pass_on(t)
+        if t < tiles - 1:
+            upto = blocks * (t + 1) // (tiles - 1)
+            score(1, done, upto)
+            done = upto
     for which, home in ((0, dp), (1, twin)):
         rows = pl.ds(pl.multiple_of(home * group, group), group)
         slices[rows, :] = normed[which, :, pl.ds(pl.multiple_of(dp * own_feats, 128), own_feats)]
         slice_copy(which, home).wait()
-    flip_out[...] = jnp.transpose(slices[...])
-
-    def wait_terms(t, _):
-        def wait(j, _):
-            term_copy(t, j).wait()
-            return 0
-
-        return lax.fori_loop(1, n, wait, 0)
-
-    lax.fori_loop(0, width // TILE, wait_terms, 0)
+    flip_buf[...] = jnp.transpose(slices[...])
+    flip_copy.start()
+    level(1)
+    wait_stats(1)
+    derive(1, twin)
+
+    passed = landed.at[pl.ds(0, line - 1)]
+    await_bytes(passed, term_recv)
+    await_bytes(passed, term_send)
+    await_bytes(crossing, cross_send)
+    my_rows = pl.ds(pl.multiple_of(me * rows_dev, rows_dev), rows_dev)
     values = normin[0, my_rows, :].astype(jnp.float32)
     inv = lax.rsqrt(jnp.mean(values * values, axis=1, keepdims=True) + norm_eps)
     dnormed = landed[0].astype(jnp.float32)
-    for slot in range(1, n):
+    for slot in range(1, line):
         dnormed += landed[slot].astype(jnp.float32)
     scaled = dnormed * gain[...]
-    input_out[...] = inv * (
+    input_buf[...] = inv * (
         scaled - values * inv * inv * jnp.mean(values * scaled, axis=1, keepdims=True)
     )
-    for which, home in ((0, dp), (1, twin)):
-        keep_copy(which, home).wait()
-        score_copy(which, home).wait()
+    input_copy.start()
+    for which in range(2):
+        await_bytes(dscore.at[which], keep_sem.at[which])
+        await_bytes(dscore.at[which], score_send.at[which])
+        await_bytes(dscore.at[which], score_recv.at[which])
     finish_units()
     finish_norm()
-
-
-def vocab_kernel(flipped, dscore, grad_input, losses, vocab_out, input_out, loss_out):
-    rows_dev = loss_out.shape[1]
+    loss_copy.wait()
+    flip_copy.wait()
+    input_copy.wait()
+
+
+def vocab_kernel(
+    flipped_in,
+    dscore_in,
+    grad_input,
+    losses_in,
+    vocab_out,
+    input_out,
+    loss_out,
+    flipped,
+    dscore,
+    results,
+    inputs,
+    losses,
+    loss_row,
+    load_sem,
+    block_sem,
+    out_sem,
+    tail_sem,
+):
+    rows_dev = loss_row.shape[1]
     group = losses.shape[1]
-    vocab_out[...] = jnp.dot(flipped[...], dscore[...], preferred_element_type=jnp.float32)
-
-    @pl.when(pl.program_id(0) == 0)
-    def _():
-        input_out[...] = grad_input[...]
-        shift = lax.rem(group - lax.axis_index("vp") * rows_dev, group)
-        loss_out[...] = pltpu.roll(losses[...], shift, 1)[0:1, :rows_dev]
+    count = dscore.shape[0]
+
+    def block_in(j):
+        cols = pl.ds(pl.multiple_of(j * BLOCK, BLOCK), BLOCK)
+        return pltpu.make_async_copy(dscore_in.at[:, cols], dscore.at[j], block_sem.at[j])
+
+    def block_out(j):
+        cols = pl.ds(pl.multiple_of(j * BLOCK, BLOCK), BLOCK)
+        return pltpu.make_async_copy(results.at[j], vocab_out.at[:, cols], out_sem.at[j])
+
+    bring = pltpu.make_async_copy(flipped_in, flipped, load_sem.at[0])
+    bring_input = pltpu.make_async_copy(grad_input, inputs, load_sem.at[1])
+    bring_losses = pltpu.make_async_copy(losses_in, losses, load_sem.at[2])
+    put_input = pltpu.make_async_copy(inputs, input_out, tail_sem.at[0])
+    put_losses = pltpu.make_async_copy(loss_row, loss_out, tail_sem.at[1])
+    bring.start()
+
+    def start_block(j, _):
+        block_in(j).start()
+        return 0
+
+    lax.fori_loop(0, count, start_block, 0)
+    bring_input.start()
+    bring_losses.start()
+    bring.wait()
+
+    def multiply(j, _):
+        block_in(j).wait()
+        results[j] = jnp.dot(flipped[...], dscore[j], preferred_element_type=jnp.float32)
+        block_out(j).start()
+        return 0
+
+    def finish(j, _):
+        block_out(j).wait()
+        return 0
+
+    lax.fori_loop(0, count // 2, multiply, 0)
+    bring_input.wait()
+    put_input.start()
+    bring_losses.wait()
+    shift = lax.rem(group - lax.axis_index("vp") * rows_dev, group)
+    loss_row[...] = pltpu.roll(losses[...], shift, 1)[0:1, :rows_dev]
+    put_losses.start()
+    lax.fori_loop(count // 2, count, multiply, 0)
+    put_input.wait()
+    put_losses.wait()
+    lax.fori_loop(0, count, finish, 0)
 
 
 def fused(stream, hidden, w_down, final_gain, vocab, vocab_bias, targets):
@@ -615,9 +773,9 @@
     ncols = vocab.shape[1]
     own_feats = width // groups
     tokens = groups * group
+    line = n // 2
     f32, bf16 = jnp.float32, jnp.bfloat16
     dma = pltpu.SemaphoreType.DMA
-    vmem = pl.BlockSpec(memory_space=pltpu.VMEM)
     hbm = pl.BlockSpec(memory_space=pl.ANY)
     group_losses, grad_input, dscore, flipped = pl.pallas_call(
         functools.partial(head_kernel, n),
@@ -627,10 +785,18 @@
             jax.ShapeDtypeStruct((tokens, ncols), bf16),
             jax.ShapeDtypeStruct((own_feats, tokens), bf16),
         ),
-        in_specs=[hbm, vmem, vmem, vmem, hbm, vmem, vmem],
-        out_specs=(vmem, vmem, hbm, vmem),
+        in_specs=[hbm] * 7,
+        out_specs=(hbm,) * 4,
         scratch_shapes=[
-            pltpu.VMEM((n, depth, group), bf16),
+            pltpu.VMEM(w_down.shape, bf16),
+            pltpu.VMEM((rows_dev, width), bf16),
+            pltpu.VMEM((1, width), f32),
+            pltpu.VMEM((1, ncols), f32),
+            pltpu.VMEM((1, group), jnp.int32),
+            pltpu.VMEM((8, group), f32),
+            pltpu.VMEM((rows_dev, width), f32),
+            pltpu.VMEM((own_feats, tokens), bf16),
+            pltpu.VMEM((n * depth, group), bf16),
             pltpu.VMEM((group, feats), bf16),
             pltpu.VMEM((2, group, width), bf16),
             pltpu.VMEM((2, group, width), bf16),
@@ -643,27 +809,31 @@
             pltpu.VMEM((group, feats), f32),
             pltpu.VMEM((2, group, ncols), bf16),
             pltpu.VMEM((tokens, own_feats), bf16),
-            pltpu.VMEM((group, width), bf16),
-            pltpu.VMEM((n, rows_dev, width), bf16),
-            dma((3, n, HALVES)),
-            dma((n, HALVES)),
-            dma((3, n, HALVES)),
-            dma((n, HALVES)),
-            dma((n,)),
-            dma((n,)),
-            dma((n, HALVES)),
-            dma((n, HALVES)),
-            dma((2, n)),
-            dma((2, n)),
+            pltpu.VMEM((line, 2, rows_dev, width), bf16),
+            pltpu.VMEM((line, rows_dev, width), bf16),
+            pltpu.VMEM((line, rows_dev, width), bf16),
+            pltpu.VMEM((line, rows_dev, width), bf16),
+            dma((3,)),
+            dma((n, UNIT_PARTS)),
+            dma((3,)),
+            dma((n, NORM_PARTS)),
+            dma,
+            dma,
+            dma,
+            dma,
             dma((2,)),
             dma((2,)),
             dma((2,)),
             dma((2,)),
-            dma((width // TILE, n)),
-            dma((width // TILE, n)),
+            dma((2,)),
+            dma((2,)),
+            dma,
+            dma((width // TILE,)),
             dma,
             dma,
+            dma((7,)),
             dma((2,)),
+            dma((3,)),
         ],
         compiler_params=pltpu.CompilerParams(
             collective_id=0, has_side_effects=True, vmem_limit_bytes=64 * 1024 * 1024 - 65536
@@ -678,28 +848,29 @@
         targets.reshape(1, group),
     )
 
-    def whole(*shape):
-        return pl.BlockSpec(shape, lambda j: (0, 0))
-
+    count = ncols // BLOCK
     grad_vocab, grad_input, losses = pl.pallas_call(
         vocab_kernel,
-        grid=(ncols // TILE,),
         out_shape=(
             jax.ShapeDtypeStruct((own_feats, ncols), f32),
             jax.ShapeDtypeStruct((rows_dev, width), f32),
             jax.ShapeDtypeStruct((1, rows_dev), f32),
         ),
-        in_specs=[
-            whole(own_feats, tokens),
-            pl.BlockSpec((tokens, TILE), lambda j: (0, j)),
-            whole(rows_dev, width),
-            whole(8, group),
+        in_specs=[hbm] * 4,
+        out_specs=(hbm,) * 3,
+        scratch_shapes=[
+            pltpu.VMEM((own_feats, tokens), bf16),
+            pltpu.VMEM((count, tokens, BLOCK), bf16),
+            pltpu.VMEM((count, own_feats, BLOCK), f32),
+            pltpu.VMEM((rows_dev, width), f32),
+            pltpu.VMEM((8, group), f32),
+            pltpu.VMEM((1, rows_dev), f32),
+            dma((3,)),
+            dma((count,)),
+            dma((count,)),
+            dma((2,)),
         ],
-        out_specs=(
-            pl.BlockSpec((own_feats, TILE), lambda j: (0, j)),
-            whole(rows_dev, width),
-            whole(1, rows_dev),
-        ),
+        compiler_params=pltpu.CompilerParams(vmem_limit_bytes=64 * 1024 * 1024 - 65536),
     )(flipped, dscore, grad_input, group_losses)
     return (losses.reshape(rows_dev), grad_input, grad_vocab)
 
@@ -712,8 +883,8 @@
         n % 2 == 0
         and groups == 4
         and rows_dev % 32 == 0
-        and depth % (16 * HALVES) == 0
-        and group % (32 * HALVES) == 0
+        and depth % (16 * UNIT_PARTS) == 0
+        and group % (32 * NORM_PARTS) == 0
         and w_down.shape[1] % 128 == 0
         and width % TILE == 0
         and (width // groups) % 128 == 0

time: 111 us -> 93.4 us (0.84)
  Pallas kernels: 110 us -> 92.6 us
    pallas_call x1, Pallas kernels: 98.4 us -> 83.9 us  [fused(): pl.pallas_call(functools.partial(head_kernel, n), out_shape=(jax.ShapeDty...]
    pallas_call x1, Pallas kernels: 11.3 us -> 8.62 us  [fused(): pl.pallas_call(vocab_kernel, out_shape=(jax.ShapeDtypeStruct((own_feats,...]
where the time goes in v1:
time: 93.4 us; the launch traced here: 93.2 us
  Pallas kernels  92.6 us (99%)
    pallas_call x1, Pallas kernels, fused(): pl.pallas_call(functools.partial(head_kernel, n), out_shape=(jax.ShapeDty...  83.9 us
    pallas_call x1, Pallas kernels, fused(): pl.pallas_call(vocab_kernel, out_shape=(jax.ShapeDtypeStruct((own_feats,...  8.62 us

profile of v1, /device:TPU:0, one launch (start us, length us, event | category | flops | bytes accessed | tf_op | source)
XLA Modules:
  0.0 93.2 jit_solution(7383253906861668610)
XLA Ops:
  0.6 83.9 %shard_map.94 = (f32[8,256]{1,0:T(8,128)}, f32[32,2048]{1,0:T(8,128)}, bf16[1024,4096]{1,0:T(8,128)(2,1)}, bf16[512,1024]{1,0:T(8,128)(2,1)}) custom-call(bf16[704,256]{1,0:T(8,128)(2,1)} %bitcast.5, bf16[5632,256]{1,0:T(8,128)(2,1)} %w_down_in.1, bf16[32,2048]{1,0:T(8,128)(2,1)} %stream_in.1, f32[1,2048]{1,0:T(1,128)} %bitcast.7, bf16[2048,4096]{1,0:T(8,128)(2,1)} %vocab.1, ...), custom_call_target="tpu_custom_call" | custom-call | tf_op jit(solution)/shard_map/pallas_call | solution.py:780
  84.6 8.6 %shard_map.95 = (f32[512,4096]{1,0:T(8,128)}, f32[32,2048]{1,0:T(8,128)}, f32[1,32]{1,0:T(1,128)}) custom-call(bf16[512,1024]{1,0:T(8,128)(2,1)} %get-tuple-element.10.flipped_in, bf16[1024,4096]{1,0:T(8,128)(2,1)} %get-tuple-element.11.dscore_in, f32[32,2048]{1,0:T(8,128)} %get-tuple-element.12.grad_input, f32[8,256]{1,0:T(8,128)} %get-tuple-element.13.losses_in), custom_call_target="tpu_custom_call" | custom-call | tf_op jit(solution)/shard_map/pallas_call | solution.py:852

commit v2 on v1

--- a/solution.py
+++ b/solution.py
@@ -92,6 +92,7 @@
 NORM_PARTS = 4
 TILE = 512
 BLOCK = 512
+AHEAD = 4
 
 
 def send(src, dst, send_sem, recv_sem, vp, dp):
@@ -242,16 +243,16 @@
     bias_in,
     targets_in,
     loss_out,
-    input_out,
+    landed,
     score_out,
     flip_out,
+    rows_out,
     w_down,
     stream,
     gain,
     bias,
     targets,
     loss_buf,
-    input_buf,
     flip_buf,
     units,
     stream_cols,
@@ -259,8 +260,12 @@
     normed,
     words,
     scores,
-    tops,
+    squared,
     lanes,
+    lines,
+    goal_ids,
+    raw,
+    stage,
     stats,
     goals,
     total,
@@ -269,7 +274,6 @@
     terms,
     crossing,
     sums,
-    landed,
     unit_send,
     unit_recv,
     norm_send,
@@ -291,6 +295,7 @@
     load_sem,
     keep_sem,
     out_sem,
+    twin_ready,
 ):
     me = lax.axis_index("vp")
     dp = lax.axis_index("dp")
@@ -312,15 +317,16 @@
 
     barrier = pltpu.get_barrier_semaphore()
 
-    def greet(j, _):
-        peer = lax.rem(me + j, n)
-        pl.semaphore_signal(barrier, 1, device_id={"vp": peer, "dp": dp}, device_id_type=MESH)
-        pl.semaphore_signal(barrier, 1, device_id={"vp": peer, "dp": twin}, device_id_type=MESH)
-        return 0
-
-    lax.fori_loop(1, n, greet, 0)
-    pl.semaphore_signal(barrier, 1, device_id={"vp": me, "dp": twin}, device_id_type=MESH)
-    pl.semaphore_signal(barrier, 1, device_id={"vp": me, "dp": sibling}, device_id_type=MESH)
+    above, below = place < line - 1, place > 0
+
+    def greet(vp, home):
+        pl.semaphore_signal(barrier, 1, device_id={"vp": vp, "dp": home}, device_id_type=MESH)
+
+    greet(me, twin)
+    greet(me, sibling)
+    greet(other, dp)
+    pl.when(above)(lambda: greet(me + 2, dp))
+    pl.when(below)(lambda: greet(me - 2, dp))
 
     def brought(at, src, dst):
         return pltpu.make_async_copy(src, dst, load_sem.at[at])
@@ -334,10 +340,9 @@
     load = brought(6, vocab, words)
     for copy in (bring, bring_stream, bring_down, bring_targets, bring_gain, bring_bias, load):
         copy.start()
-    pl.semaphore_wait(barrier, 2 * n)
-
-    def stream_copy(j):
-        peer = lax.rem(me + j, n)
+    pl.semaphore_wait(barrier, 3 + above.astype(jnp.int32) + below.astype(jnp.int32))
+
+    def stream_copy(peer):
         return send(
             stream.at[:, pl.ds(pl.multiple_of(peer * feats, 128), feats)],
             stream_cols.at[pl.ds(pl.multiple_of(me * rows_dev, rows_dev), rows_dev), :],
@@ -347,9 +352,13 @@
             dp,
         )
 
-    def start_stream(j, _):
-        stream_copy(j).start()
-        return 0
+    def pair_streams(slot, part):
+        if part == 0:
+            pl.when((lax.rem(slot, 2) == side) & (slot != me))(lambda: pair_stream(slot))
+
+    def pair_stream(slot):
+        stream_copy(slot).start()
+        stream_copy(slot + 1 - 2 * side).start()
 
     def place_units(slot, part):
         return units.at[pl.ds(pl.multiple_of(slot * depth + part * piece, 16), piece), :]
@@ -365,7 +374,7 @@
 
     def open_units():
         bring_stream.wait()
-        lax.fori_loop(1, n, start_stream, 0)
+        stream_copy(other).start()
         stream_cols[pl.ds(pl.multiple_of(me * rows_dev, rows_dev), rows_dev), :] = stream[
             :, pl.ds(pl.multiple_of(me * feats, 128), feats)
         ]
@@ -373,6 +382,7 @@
         goals[...] = jnp.transpose(
             jnp.broadcast_to(targets[...].astype(jnp.float32), (128, group))
         )
+        goal_ids[0] = goals[...].astype(jnp.int32)
         bring_down.wait()
         total[...] = product(me)
 
@@ -389,13 +399,15 @@
         place_units,
         lambda count: units.at[pl.ds(0, count * piece), :],
         (unit_send, unit_recv),
-        lambda slot, part: None,
+        pair_streams,
         open_units,
         project,
     )
     streamed = stream_cols.at[pl.ds(0, (n - 1) * rows_dev), :]
     await_bytes(streamed, stream_recv)
     await_bytes(streamed, stream_send)
+
+    pl.semaphore_signal(twin_ready, 1, device_id={"vp": me, "dp": twin}, device_id_type=MESH)
 
     def cols_of(slot):
         return pl.ds(pl.multiple_of(slot * feats, 128), feats)
@@ -416,10 +428,22 @@
     def place_norm(slot, part):
         return normin.at[0, pl.ds(part * half, half), cols_of(slot)]
 
+    def folded(pieces, join):
+        return functools.reduce(join, pieces)
+
+    def add_squares(slot):
+        values = normin[0, :, cols_of(slot)].astype(jnp.float32)
+        squares = values * values
+        squared[...] += folded([squares[:, at : at + 128] for at in range(0, feats, 128)], jnp.add)
+
     def open_norm():
+        squared[...] = jnp.zeros_like(squared)
+        add_squares(me)
         bring_gain.wait()
         bring_bias.wait()
-        tops[...] = jnp.full(tops.shape, -jnp.inf, jnp.float32)
+        lanes[0] = jnp.full((group, 128), -jnp.inf, jnp.float32)
+        lanes[1] = jnp.zeros((group, 128), jnp.float32)
+        lanes[2] = jnp.zeros((group, 128), jnp.float32)
 
     finish_norm = gather(
         n,
@@ -428,18 +452,25 @@
         NORM_PARTS,
         lambda part: place_norm(me, part),
         place_norm,
-        lambda count: scores.at[0, pl.ds(0, count * half // 8), pl.ds(0, 4 * feats)],
+        lambda count: scores.at[pl.ds(0, count * half // 8), pl.ds(0, 4 * feats)],
         (norm_send, norm_recv),
         lambda slot, part: twin_copy(slot, part).start(),
         open_norm,
-        lambda slot: None,
+        add_squares,
     )
 
     def normalize(which):
+        if which == 0:
+            mean = jnp.sum(squared[...], axis=1, keepdims=True) / width
+            squared[...] = jnp.broadcast_to(lax.rsqrt(mean + norm_eps), (group, 128))
+
         def block(j, _):
             rows = pl.ds(pl.multiple_of(j * 32, 32), 32)
             values = normin[which, rows, :].astype(jnp.float32)
-            inv = lax.rsqrt(jnp.mean(values * values, axis=1, keepdims=True) + norm_eps)
+            if which == 0:
+                inv = squared[rows, 0:1]
+            else:
+                inv = lax.rsqrt(jnp.mean(values * values, axis=1, keepdims=True) + norm_eps)
             normed[which, rows, :] = (values * inv * gain[...]).astype(jnp.bfloat16)
             return 0
 
@@ -457,45 +488,59 @@
             sibling,
         )
 
-    def folded(values, join):
-        result = values[:, :128]
-        for at in range(128, TILE, 128):
-            result = join(result, values[:, at : at + 128])
-        return result
-
-    def score(which, first, last):
-        def block(j, _):
-            cols = pl.ds(pl.multiple_of(j * TILE, TILE), TILE)
-            values = (
-                jnp.dot(normed[which], words[:, cols], preferred_element_type=jnp.float32)
-                + bias[:, cols]
-            )
-            scores[which, :, cols] = values
-            tops[which] = jnp.maximum(tops[which], folded(values, jnp.maximum))
+    def is_goal(j, at, goal):
+        ids = lax.broadcasted_iota(jnp.int32, (group, 128), 1) + (me * ncols + j * TILE + at)
+        return ids == goal
+
+    def block_cols(j):
+        return pl.ds(pl.multiple_of(j * TILE, TILE), TILE)
+
+    def piece_cols(j, i):
+        return pl.ds(pl.multiple_of(j * TILE + i * 128, 128), 128)
+
+    def multiply(which, j, slot):
+        raw[slot] = jnp.dot(
+            normed[which], words[:, block_cols(j)], preferred_element_type=jnp.float32
+        )
+
+    def raw_pieces(j, slot):
+        return [
+            raw[slot, :, at : at + 128] + bias[:, piece_cols(j, at // 128)]
+            for at in range(0, TILE, 128)
+        ]
+
+    def pairs(which, absorb, first, last, after=None):
+        def body(i, _):
+            multiply(which, 2 * i + 1, 1)
+            absorb(2 * i, 0)
+            multiply(which, 2 * i + 2, 0)
+            absorb(2 * i + 1, 1)
+            if after:
+                after(i)
             return 0
 
-        lax.fori_loop(first, last, block, 0)
-
-    def level(which):
-        top = jnp.max(tops[which], axis=1, keepdims=True)
-        tops[which] = jnp.broadcast_to(top, (group, 128))
-        lanes[...] = jnp.zeros_like(lanes)
-
-        def powers(j, _):
-            cols = pl.ds(pl.multiple_of(j * TILE, TILE), TILE)
-            values = scores[which, :, cols]
-            if which == 0:
-                ids = lax.broadcasted_iota(jnp.int32, (group, TILE), 1) + (me * ncols + j * TILE)
-                hits = jnp.where(ids == own_goals, values, 0.0)
-                lanes[1] += folded(hits, jnp.add)
-            values = jnp.exp(values - top)
-            scores[which, :, cols] = values
-            if which == 0:
-                lanes[0] += folded(values, jnp.add)
-            return 0
-
-        lax.fori_loop(0, ncols // TILE, powers, 0)
-        return top
+        final = last == blocks // 2
+        lax.fori_loop(first, last - 1 if final else last, body, 0)
+        if final:
+            multiply(which, blocks - 1, 1)
+            absorb(blocks - 2, 0)
+            absorb(blocks - 1, 1)
+            if after:
+                after(last - 1)
+
+    def absorb_own(j, slot):
+        pieces = raw_pieces(j, slot)
+        before = lanes[0]
+        peak = jnp.maximum(before, folded(pieces, jnp.maximum))
+        powers = [jnp.exp(piece - peak) for piece in pieces]
+        for i, piece in enumerate(pieces):
+            scores[:, piece_cols(j, i)] = piece
+        lanes[0] = peak
+        lanes[1] = lanes[1] * jnp.exp(before - peak) + folded(powers, jnp.add)
+        hits = [
+            jnp.where(is_goal(j, 128 * i, goal_ids[0]), piece, 0.0) for i, piece in enumerate(pieces)
+        ]
+        lanes[2] += folded(hits, jnp.add)
 
     def stat_copy(away, j, home):
         peer = lax.rem(me + j, n)
@@ -508,23 +553,24 @@
             home,
         )
 
-    own_goals = goals[:, 0:1].astype(jnp.int32)
     blocks = ncols // TILE
     normalize(0)
     load.wait()
     slice_copy(0, dp).start()
-    score(0, 0, blocks)
-    top = level(0)
+    multiply(0, 0, 0)
+    pairs(0, absorb_own, 0, blocks // 2)
+    top = jnp.max(lanes[0], axis=1, keepdims=True)
+    weight = jnp.sum(lanes[1] * jnp.exp(lanes[0] - top), axis=1, keepdims=True)
     lane = lax.broadcasted_iota(jnp.int32, (group, 128), 1)
     packed = jnp.where(
         lane == 0,
         top,
         jnp.where(
             lane == 1,
-            jnp.sum(lanes[0], axis=1, keepdims=True),
+            weight,
             jnp.where(
                 lane == 2,
-                jnp.sum(lanes[1], axis=1, keepdims=True),
+                jnp.sum(lanes[2], axis=1, keepdims=True),
                 jnp.where(lane == 3, goals[...], 0.0),
             ),
         ),
@@ -540,6 +586,7 @@
         return 0
 
     lax.fori_loop(1, n, start_stats, 0)
+    pl.semaphore_wait(twin_ready, 1)
     lax.fori_loop(0, n, start_away, 0)
 
     def wait_stats(away):
@@ -547,9 +594,12 @@
         await_bytes(arrived, stat_recv.at[away])
         await_bytes(arrived, stat_send.at[away])
 
+    def pair_cols(i):
+        return pl.ds(pl.multiple_of(i * 2 * TILE, 2 * TILE), 2 * TILE)
+
     def score_copy(which, home, j):
         rows = pl.ds(pl.multiple_of(home * group, group), group)
-        cols = pl.ds(pl.multiple_of(j * TILE, TILE), TILE)
+        cols = pair_cols(j)
         return send(
             dscore.at[which, :, cols],
             score_out.at[rows, cols],
@@ -561,16 +611,24 @@
 
     def keep_copy(which, home, j):
         rows = pl.ds(pl.multiple_of(home * group, group), group)
-        cols = pl.ds(pl.multiple_of(j * TILE, TILE), TILE)
+        cols = pair_cols(j)
         return pltpu.make_async_copy(
             dscore.at[which, :, cols], score_out.at[rows, cols], keep_sem.at[which]
         )
 
     loss_copy = pltpu.make_async_copy(loss_buf, loss_out, out_sem.at[0])
     flip_copy = pltpu.make_async_copy(flip_buf, flip_out, out_sem.at[1])
-    input_copy = pltpu.make_async_copy(input_buf, input_out, out_sem.at[2])
-
-    def derive(which, home):
+    rows_copy = pltpu.make_async_copy(
+        normin.at[0, pl.ds(pl.multiple_of(me * rows_dev, rows_dev), rows_dev), :],
+        rows_out,
+        out_sem.at[2],
+    )
+
+    def send_scores(which, home, j):
+        score_copy(which, home, j).start()
+        keep_copy(which, home, j).start()
+
+    def summary(which):
         parts = stats[which]
         highest = jnp.max(parts[:, 0, :], axis=0, keepdims=True)
         total = jnp.sum(parts[:, 1, :] * jnp.exp(parts[:, 0, :] - highest), axis=0, keepdims=True)
@@ -584,22 +642,56 @@
             jnp.where(column == 0, lse, jnp.where(column == 1, parts[0, 3:4, :], 0.0))
         )
         lse_col = turned[:, 0:1]
-        goal_col = turned[:, 1:2].astype(jnp.int32)
-        factor = jnp.exp(tops[which][:, 0:1] - lse_col) * (1.0 + 2.0 * zloss_weight * lse_col)
-
-        def block(j, _):
-            cols = pl.ds(pl.multiple_of(j * TILE, TILE), TILE)
-            ids = lax.broadcasted_iota(jnp.int32, (group, TILE), 1) + (me * ncols + j * TILE)
-            values = scores[which, :, cols] * factor - jnp.where(ids == goal_col, 1.0, 0.0)
-            dscore[which, :, cols] = values.astype(jnp.bfloat16)
-            score_copy(which, home, j).start()
-            keep_copy(which, home, j).start()
+        return lse_col, 1.0 + 2.0 * zloss_weight * lse_col, turned[:, 1:2].astype(jnp.int32)
+
+    def spread(which):
+        lse, slope, goal = summary(which)
+        lines[0] = jnp.broadcast_to(lse, (group, 128))
+        lines[1] = jnp.broadcast_to(slope, (group, 128))
+        goal_ids[which] = jnp.broadcast_to(goal, (group, 128))
+
+    def derive_own():
+        spread(0)
+
+        def derive(j, slot):
+            lse, slope, goal = lines[0], lines[1], goal_ids[0]
+            for i in range(TILE // 128):
+                hit = jnp.where(is_goal(j, 128 * i, goal), 1.0, 0.0)
+                power = jnp.exp(scores[:, piece_cols(j, i)] - lse)
+                values = (power * slope - hit).astype(jnp.bfloat16)
+                dscore[0, :, piece_cols(j, i)] = values
+                stage[slot, :, i * 128 : (i + 1) * 128] = values
+
+        def accumulate(j, slot):
+            raw[0] += lax.dot_general(
+                stage[slot],
+                words[pl.ds(0, TILE), block_cols(j)],
+                (((1,), (1,)), ((), ())),
+                preferred_element_type=jnp.float32,
+            )
+
+        def body(i, _):
+            derive(2 * i + 1, 1)
+            accumulate(2 * i, 0)
+            derive(2 * i + 2, 0)
+            accumulate(2 * i + 1, 1)
             return 0
 
-        lax.fori_loop(0, ncols // TILE, block, 0)
-
-    wait_stats(0)
-    derive(0, dp)
+        raw[0] = jnp.zeros((group, TILE), jnp.float32)
+        derive(0, 0)
+        lax.fori_loop(0, blocks // 2 - 1, body, 0)
+        derive(blocks - 1, 1)
+        accumulate(blocks - 2, 0)
+        accumulate(blocks - 1, 1)
+        put_terms(0, raw[0])
+
+    def absorb_twin(j, slot):
+        lse, slope, goal = lines[0], lines[1], goal_ids[1]
+        for i, piece in enumerate(raw_pieces(j, slot)):
+            hit = jnp.where(is_goal(j, 128 * i, goal), 1.0, 0.0)
+            values = jnp.exp(piece - lse) * slope - hit
+            dscore[1, :, piece_cols(j, i)] = values.astype(jnp.bfloat16)
+
 
     def cross_copy(t):
         cols = pl.ds(pl.multiple_of(t * TILE, TILE), TILE)
@@ -624,6 +716,11 @@
             dp,
         )
 
+    def put_terms(t, block):
+        cols = pl.ds(pl.multiple_of(t * TILE, TILE), TILE)
+        terms[:, :, :, cols] = block.astype(jnp.bfloat16).reshape(line, 2, rows_dev, TILE)
+        cross_copy(t).start()
+
     def term_block(t, _):
         cols = pl.ds(pl.multiple_of(t * TILE, TILE), TILE)
         block = lax.dot_general(
@@ -631,10 +728,15 @@
             words[cols, :],
             (((1,), (1,)), ((), ())),
             preferred_element_type=jnp.float32,
-        ).astype(jnp.bfloat16)
-        terms[:, :, :, cols] = block.reshape(line, 2, rows_dev, TILE)
-        cross_copy(t).start()
+        )
+        put_terms(t, block)
         return 0
+
+    def own_copy(t):
+        cols = pl.ds(pl.multiple_of(t * TILE, TILE), TILE)
+        return pltpu.make_async_copy(
+            sums.at[place, :, cols], landed.at[place, :, cols], out_sem.at[3]
+        )
 
     def pass_on(t):
         cols = pl.ds(t * TILE, TILE)
@@ -643,46 +745,53 @@
         sums[:, :, cols] = both.astype(jnp.bfloat16)
         for j in range(1, line):
             term_copy(t, j).start()
-        landed[place, :, cols] = sums[place, :, cols]
-
-    lax.fori_loop(0, width // TILE, term_block, 0)
+        own_copy(t).start()
+
+    rows_copy.start()
     await_bytes(normin.at[1], twin_recv)
     await_bytes(normin.at[1], twin_send)
     normalize(1)
     slice_copy(1, twin).start()
+    wait_stats(0)
+    derive_own()
     tiles = width // TILE
-    done = 0
+    lax.fori_loop(1, tiles, term_block, 0)
+    def release(first, last):
+        for i in range(blocks // 2 * first // 4, blocks // 2 * last // 4):
+            send_scores(0, dp, i)
+
+    release(0, 2)
+    wait_stats(1)
+    spread(1)
+    multiply(1, 0, 0)
+
+    def turn_slices():
+        for which, home in ((0, dp), (1, twin)):
+            rows = pl.ds(pl.multiple_of(home * group, group), group)
+            own_cols = pl.ds(pl.multiple_of(dp * own_feats, 128), own_feats)
+            slices[rows, :] = normed[which, :, own_cols]
+            slice_copy(which, home).wait()
+        flip_buf[...] = jnp.transpose(slices[...])
+        flip_copy.start()
+
+    def score_twin(first, last):
+        pairs(1, absorb_twin, first, last, lambda i: send_scores(1, twin, i))
+
+    halfway = blocks // 4
     for t in range(tiles):
         pass_on(t)
-        if t < tiles - 1:
-            upto = blocks * (t + 1) // (tiles - 1)
-            score(1, done, upto)
-            done = upto
-    for which, home in ((0, dp), (1, twin)):
-        rows = pl.ds(pl.multiple_of(home * group, group), group)
-        slices[rows, :] = normed[which, :, pl.ds(pl.multiple_of(dp * own_feats, 128), own_feats)]
-        slice_copy(which, home).wait()
-    flip_buf[...] = jnp.transpose(slices[...])
-    flip_copy.start()
-    level(1)
-    wait_stats(1)
-    derive(1, twin)
-
-    passed = landed.at[pl.ds(0, line - 1)]
+        if t < 2:
+            release(2 + t, 3 + t)
+        if t < tiles - 2:
+            score_twin(halfway * t // (tiles - 2), halfway * (t + 1) // (tiles - 2))
+        elif t == tiles - 2:
+            turn_slices()
+    score_twin(halfway, blocks // 2)
+    passed = sums.at[pl.ds(0, line - 1)]
     await_bytes(passed, term_recv)
     await_bytes(passed, term_send)
     await_bytes(crossing, cross_send)
-    my_rows = pl.ds(pl.multiple_of(me * rows_dev, rows_dev), rows_dev)
-    values = normin[0, my_rows, :].astype(jnp.float32)
-    inv = lax.rsqrt(jnp.mean(values * values, axis=1, keepdims=True) + norm_eps)
-    dnormed = landed[0].astype(jnp.float32)
-    for slot in range(1, line):
-        dnormed += landed[slot].astype(jnp.float32)
-    scaled = dnormed * gain[...]
-    input_buf[...] = inv * (
-        scaled - values * inv * inv * jnp.mean(values * scaled, axis=1, keepdims=True)
-    )
-    input_copy.start()
+    await_bytes(sums.at[0], out_sem.at[3])
     for which in range(2):
         await_bytes(dscore.at[which], keep_sem.at[which])
         await_bytes(dscore.at[which], score_send.at[which])
@@ -691,13 +800,15 @@
     finish_norm()
     loss_copy.wait()
     flip_copy.wait()
-    input_copy.wait()
+    rows_copy.wait()
 
 
 def vocab_kernel(
     flipped_in,
     dscore_in,
-    grad_input,
+    landed_in,
+    rows_in,
+    gain_in,
     losses_in,
     vocab_out,
     input_out,
@@ -705,6 +816,9 @@
     flipped,
     dscore,
     results,
+    landed,
+    rows,
+    gain,
     inputs,
     losses,
     loss_row,
@@ -725,43 +839,101 @@
         cols = pl.ds(pl.multiple_of(j * BLOCK, BLOCK), BLOCK)
         return pltpu.make_async_copy(results.at[j], vocab_out.at[:, cols], out_sem.at[j])
 
-    bring = pltpu.make_async_copy(flipped_in, flipped, load_sem.at[0])
-    bring_input = pltpu.make_async_copy(grad_input, inputs, load_sem.at[1])
-    bring_losses = pltpu.make_async_copy(losses_in, losses, load_sem.at[2])
+    loads = [
+        pltpu.make_async_copy(src, dst, load_sem.at[i])
+        for i, (src, dst) in enumerate(
+            [
+                (flipped_in, flipped),
+                (landed_in, landed),
+                (rows_in, rows),
+                (gain_in, gain),
+                (losses_in, losses),
+            ]
+        )
+    ]
     put_input = pltpu.make_async_copy(inputs, input_out, tail_sem.at[0])
     put_losses = pltpu.make_async_copy(loss_row, loss_out, tail_sem.at[1])
-    bring.start()
-
-    def start_block(j, _):
+    loads[0].start()
+    block_in(0).start()
+    for load in loads[1:]:
+        load.start()
+    for j in range(1, min(AHEAD, count)):
         block_in(j).start()
-        return 0
-
-    lax.fori_loop(0, count, start_block, 0)
-    bring_input.start()
-    bring_losses.start()
-    bring.wait()
 
     def multiply(j, _):
+        @pl.when(j + AHEAD - 1 < count)
+        def _():
+            block_in(j + AHEAD - 1).start()
+
         block_in(j).wait()
         results[j] = jnp.dot(flipped[...], dscore[j], preferred_element_type=jnp.float32)
         block_out(j).start()
         return 0
 
+    for load in loads:
+        load.wait()
+    block_in(0).wait()
+    results[0] = jnp.dot(flipped[...], dscore[0], preferred_element_type=jnp.float32)
+    values = rows[...].astype(jnp.float32)
+    inv = lax.rsqrt(jnp.mean(values * values, axis=1, keepdims=True) + norm_eps)
+    dnormed = landed[0].astype(jnp.float32)
+    for slot in range(1, landed.shape[0]):
+        dnormed += landed[slot].astype(jnp.float32)
+    scaled = dnormed * gain[...]
+    inputs[...] = inv * (
+        scaled - values * inv * inv * jnp.mean(values * scaled, axis=1, keepdims=True)
+    )
+    shift = lax.rem(group - lax.axis_index("vp") * rows_dev, group)
+    loss_row[...] = pltpu.roll(losses[...], shift, 1)[0:1, :rows_dev]
+    block_out(0).start()
+    put_input.start()
+    put_losses.start()
+
     def finish(j, _):
         block_out(j).wait()
         return 0
 
-    lax.fori_loop(0, count // 2, multiply, 0)
-    bring_input.wait()
-    put_input.start()
-    bring_losses.wait()
-    shift = lax.rem(group - lax.axis_index("vp") * rows_dev, group)
-    loss_row[...] = pltpu.roll(losses[...], shift, 1)[0:1, :rows_dev]
-    put_losses.start()
-    lax.fori_loop(count // 2, count, multiply, 0)
+    lax.fori_loop(1, count, multiply, 0)
     put_input.wait()
     put_losses.wait()
     lax.fori_loop(0, count, finish, 0)
+
+
+def vocab_call(flipped, dscore, landed, rows, gain, group_losses):
+    own_feats, tokens = flipped.shape
+    ncols = dscore.shape[1]
+    line, rows_dev, width = landed.shape
+    group = group_losses.shape[1]
+    f32, bf16 = jnp.float32, jnp.bfloat16
+    dma = pltpu.SemaphoreType.DMA
+    hbm = pl.BlockSpec(memory_space=pl.ANY)
+    count = ncols // BLOCK
+    return pl.pallas_call(
+        vocab_kernel,
+        out_shape=(
+            jax.ShapeDtypeStruct((own_feats, ncols), f32),
+            jax.ShapeDtypeStruct((rows_dev, width), f32),
+            jax.ShapeDtypeStruct((1, rows_dev), f32),
+        ),
+        in_specs=[hbm] * 6,
+        out_specs=(hbm,) * 3,
+        scratch_shapes=[
+            pltpu.VMEM((own_feats, tokens), bf16),
+            pltpu.VMEM((count, tokens, BLOCK), bf16),
+            pltpu.VMEM((count, own_feats, BLOCK), f32),
+            pltpu.VMEM((line, rows_dev, width), bf16),
+            pltpu.VMEM((rows_dev, width), bf16),
+            pltpu.VMEM((1, width), f32),
+            pltpu.VMEM((rows_dev, width), f32),
+            pltpu.VMEM((8, group), f32),
+            pltpu.VMEM((1, rows_dev), f32),
+            dma((5,)),
+            dma((count,)),
+            dma((count,)),
+            dma((2,)),
+        ],
+        compiler_params=pltpu.CompilerParams(vmem_limit_bytes=64 * 1024 * 1024 - 65536),
+    )(flipped, dscore, landed, rows, gain, group_losses)
 
 
 def fused(stream, hidden, w_down, final_gain, vocab, vocab_bias, targets):
@@ -777,16 +949,18 @@
     f32, bf16 = jnp.float32, jnp.bfloat16
     dma = pltpu.SemaphoreType.DMA
     hbm = pl.BlockSpec(memory_space=pl.ANY)
-    group_losses, grad_input, dscore, flipped = pl.pallas_call(
+    gain = final_gain.reshape(1, width)
+    group_losses, landed, dscore, flipped, rows = pl.pallas_call(
         functools.partial(head_kernel, n),
         out_shape=(
             jax.ShapeDtypeStruct((8, group), f32),
-            jax.ShapeDtypeStruct((rows_dev, width), f32),
+            jax.ShapeDtypeStruct((line, rows_dev, width), bf16),
             jax.ShapeDtypeStruct((tokens, ncols), bf16),
             jax.ShapeDtypeStruct((own_feats, tokens), bf16),
+            jax.ShapeDtypeStruct((rows_dev, width), bf16),
         ),
         in_specs=[hbm] * 7,
-        out_specs=(hbm,) * 4,
+        out_specs=(hbm,) * 5,
         scratch_shapes=[
             pltpu.VMEM(w_down.shape, bf16),
             pltpu.VMEM((rows_dev, width), bf16),
@@ -794,23 +968,25 @@
             pltpu.VMEM((1, ncols), f32),
             pltpu.VMEM((1, group), jnp.int32),
             pltpu.VMEM((8, group), f32),
-            pltpu.VMEM((rows_dev, width), f32),
             pltpu.VMEM((own_feats, tokens), bf16),
             pltpu.VMEM((n * depth, group), bf16),
             pltpu.VMEM((group, feats), bf16),
             pltpu.VMEM((2, group, width), bf16),
             pltpu.VMEM((2, group, width), bf16),
             pltpu.VMEM((width, ncols), bf16),
-            pltpu.VMEM((2, group, ncols), f32),
+            pltpu.VMEM((group, ncols), f32),
+            pltpu.VMEM((group, 128), f32),
+            pltpu.VMEM((3, group, 128), f32),
             pltpu.VMEM((2, group, 128), f32),
-            pltpu.VMEM((2, group, 128), f32),
+            pltpu.VMEM((2, group, 128), jnp.int32),
+            pltpu.VMEM((2, group, TILE), f32),
+            pltpu.VMEM((2, group, TILE), bf16),
             pltpu.VMEM((2, n, 8, group), f32),
             pltpu.VMEM((group, 128), f32),
             pltpu.VMEM((group, feats), f32),
             pltpu.VMEM((2, group, ncols), bf16),
             pltpu.VMEM((tokens, own_feats), bf16),
             pltpu.VMEM((line, 2, rows_dev, width), bf16),
-            pltpu.VMEM((line, rows_dev, width), bf16),
             pltpu.VMEM((line, rows_dev, width), bf16),
             pltpu.VMEM((line, rows_dev, width), bf16),
             dma((3,)),
@@ -833,7 +1009,8 @@
             dma,
             dma((7,)),
             dma((2,)),
-            dma((3,)),
+            dma((4,)),
+            pltpu.SemaphoreType.REGULAR,
         ],
         compiler_params=pltpu.CompilerParams(
             collective_id=0, has_side_effects=True, vmem_limit_bytes=64 * 1024 * 1024 - 65536
@@ -842,36 +1019,13 @@
         hidden.T,
         w_down,
         stream,
-        final_gain.reshape(1, width),
+        gain,
         vocab,
         vocab_bias.reshape(1, ncols),
         targets.reshape(1, group),
     )
 
-    count = ncols // BLOCK
-    grad_vocab, grad_input, losses = pl.pallas_call(
-        vocab_kernel,
-        out_shape=(
-            jax.ShapeDtypeStruct((own_feats, ncols), f32),
-            jax.ShapeDtypeStruct((rows_dev, width), f32),
-            jax.ShapeDtypeStruct((1, rows_dev), f32),
-        ),
-        in_specs=[hbm] * 4,
-        out_specs=(hbm,) * 3,
-        scratch_shapes=[
-            pltpu.VMEM((own_feats, tokens), bf16),
-            pltpu.VMEM((count, tokens, BLOCK), bf16),
-            pltpu.VMEM((count, own_feats, BLOCK), f32),
-            pltpu.VMEM((rows_dev, width), f32),
-            pltpu.VMEM((8, group), f32),
-            pltpu.VMEM((1, rows_dev), f32),
-            dma((3,)),
-            dma((count,)),
-            dma((count,)),
-            dma((2,)),
-        ],
-        compiler_params=pltpu.CompilerParams(vmem_limit_bytes=64 * 1024 * 1024 - 65536),
-    )(flipped, dscore, grad_input, group_losses)
+    grad_vocab, grad_input, losses = vocab_call(flipped, dscore, landed, rows, gain, group_losses)
     return (losses.reshape(rows_dev), grad_input, grad_vocab)
 
 
@@ -888,7 +1042,7 @@
         and w_down.shape[1] % 128 == 0
         and width % TILE == 0
         and (width // groups) % 128 == 0
-        and vocab.shape[1] % TILE == 0
+        and vocab.shape[1] % (2 * TILE) == 0
     )
     path = fused if tiles else body
     return path(stream, hidden, w_down, final_gain, vocab, vocab_bias, targets)

time: 93.4 us -> 89.1 us (0.954)
  Pallas kernels: 92.6 us -> 88.2 us
    pallas_call x1, Pallas kernels: 83.9 us -> 79.1 us  [fused(): pl.pallas_call(functools.partial(head_kernel, n), out_shape=(jax.ShapeDty...]
where the time goes in v2:
time: 89.1 us; the launch traced here: 89 us
  Pallas kernels  88.2 us (99%)
    pallas_call x1, Pallas kernels, fused(): pl.pallas_call(functools.partial(head_kernel, n), out_shape=(jax.ShapeDty...  79.1 us
    pallas_call x1, Pallas kernels, vocab_call(): pl.pallas_call(vocab_kernel, out_shape=(jax.ShapeDtypeStruct((own_feats,...  9.07 us

profile of v2, /device:TPU:0, one launch (start us, length us, event | category | flops | bytes accessed | tf_op | source)
XLA Modules:
  0.0 89.0 jit_solution(17194667149562671878)
XLA Ops:
  0.6 79.1 %shard_map.94 = (f32[8,256]{1,0:T(8,128)}, bf16[4,32,2048]{2,1,0:T(8,128)(2,1)}, bf16[1024,4096]{1,0:T(8,128)(2,1)}, bf16[512,1024]{1,0:T(8,128)(2,1)}, bf16[32,2048]{1,0:T(8,128)(2,1)}) custom-call(bf16[704,256]{1,0:T(8,128)(2,1)} %bitcast.5, bf16[5632,256]{1,0:T(8,128)(2,1)} %w_down_in.1, bf16[32,2048]{1,0:T(8,128)(2,1)} %stream_in.1, f32[1,2048]{1,0:T(1,128)} %bitcast.6, ...), custom_call_target="tpu_custom_call" | custom-call | tf_op jit(solution)/shard_map/pallas_call | solution.py:953
  79.7 9.1 %shard_map.95 = (f32[512,4096]{1,0:T(8,128)}, f32[32,2048]{1,0:T(8,128)}, f32[1,32]{1,0:T(1,128)}) custom-call(bf16[512,1024]{1,0:T(8,128)(2,1)} %get-tuple-element.11.flipped_in, bf16[1024,4096]{1,0:T(8,128)(2,1)} %get-tuple-element.12.dscore_in, bf16[4,32,2048]{2,1,0:T(8,128)(2,1)} %get-tuple-element.13.landed_in, ...), custom_call_target="tpu_custom_call" | custom-call | tf_op jit(solution)/shard_map/pallas_call | solution.py:911

commit v3 on v2

--- a/solution.py
+++ b/solution.py
@@ -106,7 +106,7 @@
     )
 
 
-def gather(n, me, dp, parts, own, place, bulk, sems, extra, first, use):
+def gather(n, me, dp, parts, own, place, bulk, sems, extra, first, use, between):
     line = n // 2
     here = me // 2
     side = me - 2 * here
@@ -209,6 +209,7 @@
         for part in range(parts):
             straight(k, part, -k, 1)
             straight(k, part, k, 2)
+            between(k, part)
         if k > 1:
             routed(k - 1)
         crossed(k - 1)
@@ -266,6 +267,7 @@
     goal_ids,
     raw,
     stage,
+    picked,
     stats,
     goals,
     total,
@@ -312,6 +314,8 @@
     rows_dev = stream.shape[0]
     ncols = bias.shape[1]
     own_feats = slices.shape[1]
+    blocks = ncols // TILE
+    tiles = width // TILE
     half = group // NORM_PARTS
     piece = depth // UNIT_PARTS
 
@@ -372,6 +376,34 @@
             preferred_element_type=jnp.float32,
         )
 
+    def is_goal(j, at, goal):
+        ids = lax.broadcasted_iota(jnp.int32, (group, 128), 1) + (me * ncols + j * TILE + at)
+        return ids == goal
+
+    def block_cols(j):
+        return pl.ds(pl.multiple_of(j * TILE, TILE), TILE)
+
+    def piece_cols(j, i):
+        return pl.ds(pl.multiple_of(j * TILE + i * 128, 128), 128)
+
+    def times_vocab(left, t):
+        return lax.dot_general(
+            left, words[block_cols(t), :], (((1,), (1,)), ((), ())), preferred_element_type=jnp.float32
+        )
+
+    def pick_targets(k, part):
+        if k == 1 and part == 0:
+            load.wait()
+
+        def pick(t, _):
+            picked[:, block_cols(t)] = times_vocab(dscore[0], t).astype(jnp.bfloat16)
+            return 0
+
+        rounds = min(2, line - 1) * UNIT_PARTS
+        at = (k - 1) * UNIT_PARTS + part
+        if at < rounds:
+            lax.fori_loop(tiles * at // rounds, tiles * (at + 1) // rounds, pick, 0)
+
     def open_units():
         bring_stream.wait()
         stream_copy(other).start()
@@ -383,6 +415,14 @@
             jnp.broadcast_to(targets[...].astype(jnp.float32), (128, group))
         )
         goal_ids[0] = goals[...].astype(jnp.int32)
+
+        def mark(j, _):
+            for i in range(TILE // 128):
+                hit = jnp.where(is_goal(j, 128 * i, goal_ids[0]), 1.0, 0.0)
+                dscore[0, :, piece_cols(j, i)] = hit.astype(jnp.bfloat16)
+            return 0
+
+        lax.fori_loop(0, blocks, mark, 0)
         bring_down.wait()
         total[...] = product(me)
 
@@ -402,6 +442,7 @@
         pair_streams,
         open_units,
         project,
+        pick_targets,
     )
     streamed = stream_cols.at[pl.ds(0, (n - 1) * rows_dev), :]
     await_bytes(streamed, stream_recv)
@@ -457,6 +498,7 @@
         lambda slot, part: twin_copy(slot, part).start(),
         open_norm,
         add_squares,
+        lambda k, part: None,
     )
 
     def normalize(which):
@@ -488,16 +530,6 @@
             sibling,
         )
 
-    def is_goal(j, at, goal):
-        ids = lax.broadcasted_iota(jnp.int32, (group, 128), 1) + (me * ncols + j * TILE + at)
-        return ids == goal
-
-    def block_cols(j):
-        return pl.ds(pl.multiple_of(j * TILE, TILE), TILE)
-
-    def piece_cols(j, i):
-        return pl.ds(pl.multiple_of(j * TILE + i * 128, 128), 128)
-
     def multiply(which, j, slot):
         raw[slot] = jnp.dot(
             normed[which], words[:, block_cols(j)], preferred_element_type=jnp.float32
@@ -516,7 +548,8 @@
             multiply(which, 2 * i + 2, 0)
             absorb(2 * i + 1, 1)
             if after:
-                after(i)
+                after(2 * i)
+                after(2 * i + 1)
             return 0
 
         final = last == blocks // 2
@@ -524,9 +557,11 @@
         if final:
             multiply(which, blocks - 1, 1)
             absorb(blocks - 2, 0)
+            if after:
+                after(blocks - 2)
             absorb(blocks - 1, 1)
             if after:
-                after(last - 1)
+                after(blocks - 1)
 
     def absorb_own(j, slot):
         pieces = raw_pieces(j, slot)
@@ -553,14 +588,13 @@
             home,
         )
 
-    blocks = ncols // TILE
     normalize(0)
-    load.wait()
     slice_copy(0, dp).start()
     multiply(0, 0, 0)
     pairs(0, absorb_own, 0, blocks // 2)
     top = jnp.max(lanes[0], axis=1, keepdims=True)
     weight = jnp.sum(lanes[1] * jnp.exp(lanes[0] - top), axis=1, keepdims=True)
+    lanes[0] = jnp.broadcast_to(top, (group, 128))
     lane = lax.broadcasted_iota(jnp.int32, (group, 128), 1)
     packed = jnp.where(
         lane == 0,
@@ -594,12 +628,9 @@
         await_bytes(arrived, stat_recv.at[away])
         await_bytes(arrived, stat_send.at[away])
 
-    def pair_cols(i):
-        return pl.ds(pl.multiple_of(i * 2 * TILE, 2 * TILE), 2 * TILE)
-
     def score_copy(which, home, j):
         rows = pl.ds(pl.multiple_of(home * group, group), group)
-        cols = pair_cols(j)
+        cols = block_cols(j)
         return send(
             dscore.at[which, :, cols],
             score_out.at[rows, cols],
@@ -611,7 +642,7 @@
 
     def keep_copy(which, home, j):
         rows = pl.ds(pl.multiple_of(home * group, group), group)
-        cols = pair_cols(j)
+        cols = block_cols(j)
         return pltpu.make_async_copy(
             dscore.at[which, :, cols], score_out.at[rows, cols], keep_sem.at[which]
         )
@@ -650,15 +681,10 @@
         lines[1] = jnp.broadcast_to(slope, (group, 128))
         goal_ids[which] = jnp.broadcast_to(goal, (group, 128))
 
-    def derive_own():
-        spread(0)
-
-        def derive(j, slot):
-            lse, slope, goal = lines[0], lines[1], goal_ids[0]
+    def first_terms():
+        def power(j, slot):
             for i in range(TILE // 128):
-                hit = jnp.where(is_goal(j, 128 * i, goal), 1.0, 0.0)
-                power = jnp.exp(scores[:, piece_cols(j, i)] - lse)
-                values = (power * slope - hit).astype(jnp.bfloat16)
+                values = jnp.exp(scores[:, piece_cols(j, i)] - lanes[0]).astype(jnp.bfloat16)
                 dscore[0, :, piece_cols(j, i)] = values
                 stage[slot, :, i * 128 : (i + 1) * 128] = values
 
@@ -671,19 +697,29 @@
             )
 
         def body(i, _):
-            derive(2 * i + 1, 1)
+            power(2 * i + 1, 1)
             accumulate(2 * i, 0)
-            derive(2 * i + 2, 0)
+            power(2 * i + 2, 0)
             accumulate(2 * i + 1, 1)
             return 0
 
         raw[0] = jnp.zeros((group, TILE), jnp.float32)
-        derive(0, 0)
+        power(0, 0)
         lax.fori_loop(0, blocks // 2 - 1, body, 0)
-        derive(blocks - 1, 1)
+        power(blocks - 1, 1)
         accumulate(blocks - 2, 0)
         accumulate(blocks - 1, 1)
-        put_terms(0, raw[0])
+
+    def derive_own():
+        def block(j, _):
+            lse, slope, goal = lines[0], lines[1], goal_ids[0]
+            for i in range(TILE // 128):
+                hit = jnp.where(is_goal(j, 128 * i, goal), 1.0, 0.0)
+                power = jnp.exp(scores[:, piece_cols(j, i)] - lse)
+                dscore[0, :, piece_cols(j, i)] = (power * slope - hit).astype(jnp.bfloat16)
+            return 0
+
+        lax.fori_loop(0, blocks, block, 0)
 
     def absorb_twin(j, slot):
         lse, slope, goal = lines[0], lines[1], goal_ids[1]
@@ -717,19 +753,16 @@
         )
 
     def put_terms(t, block):
-        cols = pl.ds(pl.multiple_of(t * TILE, TILE), TILE)
-        terms[:, :, :, cols] = block.astype(jnp.bfloat16).reshape(line, 2, rows_dev, TILE)
+        for i in range(TILE // 128):
+            values = block[:, i * 128 : (i + 1) * 128] * lanes[1]
+            values -= picked[:, piece_cols(t, i)].astype(jnp.float32)
+            terms[:, :, :, piece_cols(t, i)] = values.astype(jnp.bfloat16).reshape(
+                line, 2, rows_dev, 128
+            )
         cross_copy(t).start()
 
     def term_block(t, _):
-        cols = pl.ds(pl.multiple_of(t * TILE, TILE), TILE)
-        block = lax.dot_general(
-            dscore[0],
-            words[cols, :],
-            (((1,), (1,)), ((), ())),
-            preferred_element_type=jnp.float32,
-        )
-        put_terms(t, block)
+        put_terms(t, times_vocab(dscore[0], t))
         return 0
 
     def own_copy(t):
@@ -748,22 +781,23 @@
         own_copy(t).start()
 
     rows_copy.start()
+    first_terms()
+    raw[1] = times_vocab(dscore[0], 1)
     await_bytes(normin.at[1], twin_recv)
     await_bytes(normin.at[1], twin_send)
     normalize(1)
     slice_copy(1, twin).start()
     wait_stats(0)
-    derive_own()
-    tiles = width // TILE
-    lax.fori_loop(1, tiles, term_block, 0)
+    spread(0)
+    lanes[1] = jnp.exp(lanes[0] - lines[0]) * lines[1]
+    put_terms(0, raw[0])
+    put_terms(1, raw[1])
+    lax.fori_loop(2, tiles, term_block, 0)
+
     def release(first, last):
         for i in range(blocks // 2 * first // 4, blocks // 2 * last // 4):
-            send_scores(0, dp, i)
-
-    release(0, 2)
-    wait_stats(1)
-    spread(1)
-    multiply(1, 0, 0)
+            send_scores(0, dp, 2 * i)
+            send_scores(0, dp, 2 * i + 1)
 
     def turn_slices():
         for which, home in ((0, dp), (1, twin)):
@@ -775,18 +809,21 @@
         flip_copy.start()
 
     def score_twin(first, last):
-        pairs(1, absorb_twin, first, last, lambda i: send_scores(1, twin, i))
-
-    halfway = blocks // 4
+        pairs(1, absorb_twin, first, last, lambda j: send_scores(1, twin, j))
+
+    pieces = blocks // 2
+    derive_own()
+    wait_stats(1)
+    spread(1)
+    multiply(1, 0, 0)
     for t in range(tiles):
+        if t == tiles - 1:
+            turn_slices()
         pass_on(t)
         if t < 2:
-            release(2 + t, 3 + t)
-        if t < tiles - 2:
-            score_twin(halfway * t // (tiles - 2), halfway * (t + 1) // (tiles - 2))
-        elif t == tiles - 2:
-            turn_slices()
-    score_twin(halfway, blocks // 2)
+            release(2 * t, 2 * t + 2)
+            score_twin(pieces * t // 4, pieces * (t + 1) // 4)
+    score_twin(pieces // 2, pieces)
     passed = sums.at[pl.ds(0, line - 1)]
     await_bytes(passed, term_recv)
     await_bytes(passed, term_send)
@@ -981,6 +1018,7 @@
             pltpu.VMEM((2, group, 128), jnp.int32),
             pltpu.VMEM((2, group, TILE), f32),
             pltpu.VMEM((2, group, TILE), bf16),
+            pltpu.VMEM((group, width), bf16),
             pltpu.VMEM((2, n, 8, group), f32),
             pltpu.VMEM((group, 128), f32),
             pltpu.VMEM((group, feats), f32),
@@ -1035,14 +1073,16 @@
     n, groups = lax.axis_size("vp"), lax.axis_size("dp")
     tiles = (
         n % 2 == 0
+        and n >= 4
         and groups == 4
         and rows_dev % 32 == 0
         and depth % (16 * UNIT_PARTS) == 0
         and group % (32 * NORM_PARTS) == 0
         and w_down.shape[1] % 128 == 0
         and width % TILE == 0
+        and width >= 4 * TILE
         and (width // groups) % 128 == 0
-        and vocab.shape[1] % (2 * TILE) == 0
+        and vocab.shape[1] % (8 * TILE) == 0
     )
     path = fused if tiles else body
     return path(stream, hidden, w_down, final_gain, vocab, vocab_bias, targets)

time: 89.1 us -> 87.3 us (0.980)
  Pallas kernels: 88.2 us -> 86.3 us
    pallas_call x1, Pallas kernels: 79.1 us -> 77.2 us  [fused(): pl.pallas_call(functools.partial(head_kernel, n), out_shape=(jax.ShapeDty...]
where the time goes in v3:
time: 87.3 us; the launch traced here: 87.1 us
  Pallas kernels  86.3 us (99%)
    pallas_call x1, Pallas kernels, fused(): pl.pallas_call(functools.partial(head_kernel, n), out_shape=(jax.ShapeDty...  77.2 us
    pallas_call x1, Pallas kernels, vocab_call(): pl.pallas_call(vocab_kernel, out_shape=(jax.ShapeDtypeStruct((own_feats,...  9.07 us

profile of v3, /device:TPU:0, one launch (start us, length us, event | category | flops | bytes accessed | tf_op | source)
XLA Modules:
  0.0 87.1 jit_solution(13605319087506665516)
XLA Ops:
  0.6 77.2 %shard_map.94 = (f32[8,256]{1,0:T(8,128)}, bf16[4,32,2048]{2,1,0:T(8,128)(2,1)}, bf16[1024,4096]{1,0:T(8,128)(2,1)}, bf16[512,1024]{1,0:T(8,128)(2,1)}, bf16[32,2048]{1,0:T(8,128)(2,1)}) custom-call(bf16[704,256]{1,0:T(8,128)(2,1)} %bitcast.5, bf16[5632,256]{1,0:T(8,128)(2,1)} %w_down_in.1, bf16[32,2048]{1,0:T(8,128)(2,1)} %stream_in.1, f32[1,2048]{1,0:T(1,128)} %bitcast.6, ...), custom_call_target="tpu_custom_call" | custom-call | tf_op jit(solution)/shard_map/pallas_call | solution.py:990
  77.9 9.1 %shard_map.95 = (f32[512,4096]{1,0:T(8,128)}, f32[32,2048]{1,0:T(8,128)}, f32[1,32]{1,0:T(1,128)}) custom-call(bf16[512,1024]{1,0:T(8,128)(2,1)} %get-tuple-element.11.flipped_in, bf16[1024,4096]{1,0:T(8,128)(2,1)} %get-tuple-element.12.dscore_in, bf16[4,32,2048]{2,1,0:T(8,128)(2,1)} %get-tuple-element.13.landed_in, ...), custom_call_target="tpu_custom_call" | custom-call | tf_op jit(solution)/shard_map/pallas_call | solution.py:948
